TPU v7x, 512 devices: a whole 4x4x16 slice. The times are simulated.
512 devices in a mesh: ep: 32 (over z, core), tp: 16 (over y, x).
Axes of the slice: x: 4, y: 4, z: 16, core: 2. Of those that a mesh axis runs over, the one named last changes fastest.
Arguments:
- branch_in: bfloat16 [131072, 512], P(('ep', 'tp')), may hold values from -6 to 6
- pool_weight: bfloat16 [4, 128, 128], replicated, may hold values from -0.5 to 0.5
- group_gain: float32 [512], replicated, may hold values from 0.1 to 1.9
- out_weight: bfloat16 [512, 2048], P(None, 'tp'), may hold values from -0.25 to 0.25
- out_gain: float32 [2048], replicated, may hold values from 0.1 to 1.9
- ffn_input: bfloat16 [4096, 2048], P('ep'), may hold values from -6 to 6
- ffn_gain: float32 [2048], replicated, may hold values from 0.1 to 1.9
- routes: int32 [4096, 4], P('ep'), may hold values from 0 to 31, all different within a row; in each aligned block of 128 rows (0 to 127, 128 to 255, ...) at most 32 rows name the same one
- route_weight: float32 [4096, 4], P('ep'), may hold values from 0.2 to 2
- gate_weight: bfloat16 [32, 2048, 4096], P('ep', None, 'tp'), may hold values from -0.375 to 0.375
- up_weight: bfloat16 [32, 2048, 4096], P('ep', None, 'tp'), may hold values from -0.375 to 0.375
- down_weight: bfloat16 [32, 4096, 2048], P('ep', 'tp'), may hold values from -0.0078125 to 0.0078125
Outputs:
- mixer_out: bfloat16 [131072, 2048], P(('ep', 'tp'))
- expert_out: bfloat16 [4096, 2048], P('ep', 'tp')
Inputs may be any that keep to these rules, and one draw needn't show every extreme that they name: `routes`: each row names 4 different experts. Among the 128 rows of one index of ep no expert is named by more than 32 rows, and in some such block one expert is named by exactly 32.
All inputs are finite; a program needn't handle non-finite values.
Results may differ from a plain program's by a relative error of at most 0.017.
Values may be sent and summed in bfloat16 or wider, within the bound.
A program may use at most 64 MiB of HBM per device.

v0:
```python
import jax
import jax.numpy as jnp
from jax import lax
from jax.sharding import Mesh
from jax.sharding import PartitionSpec as P

EP_TP = ("ep_0", "ep_1", "tp")
EP = ("ep_0", "ep_1")


pool_windows = (2, 4, 8, 16)
rim_rows = 15
norm_eps = 1e-06
clamp_limit = 7.0
sigmoid_slope = 1.702


def shifted_2(block, axis, distance):
    devices = range(lax.axis_size(axis))
    route = [(i - distance, i) for i in devices if i - distance in devices]
    return lax.ppermute(block, axis, route)


def in_order(parts, dim):
    parts = jnp.moveaxis(parts, 0, dim)
    shape = parts.shape
    return parts.reshape(*shape[:dim], shape[dim] * shape[dim + 1], *shape[dim + 2 :])


def from_everyone(shard, axis):
    devices = lax.axis_size(axis)
    return lax.all_to_all(
        jnp.broadcast_to(shard[None], (devices, *shard.shape)), axis, 0, 0, tiled=True
    )


def gathered_copies(shard, axis, dim):
    return in_order(from_everyone(shard, axis), dim)


def in_blocks(shard, dim, devices):
    before, after = (shard.shape[:dim], shard.shape[dim + 1 :])
    return jnp.moveaxis(shard.reshape(*before, devices, -1, *after), dim, 0)


def sent_and_summed(shard, axis, dim):
    devices = lax.axis_size(axis)
    parts = lax.all_to_all(in_blocks(shard, dim, devices), axis, 0, 0, tiled=True)
    return jnp.sum(parts.astype(jnp.float32), axis=0)


def exchange_in_order(parts, axes, sequence):
    inside = parts.shape[1:]
    filled = parts.reshape(*(lax.axis_size(a) for a in axes), *inside)
    for k in sequence:
        filled = lax.all_to_all(filled, axes[k], k, k, tiled=True)
    return filled.reshape(-1, *inside)


def exchange_by_chip(shard, groups, sequence, split_dim, concat_dim):
    devices = lax.axis_size(groups[0]) * lax.axis_size(groups[1])
    parts = in_blocks(shard, split_dim, devices)
    return in_order(exchange_in_order(parts, groups, sequence), concat_dim)


def rms_scale(values, gain):
    return values * lax.rsqrt(jnp.mean(values * values, axis=-1, keepdims=True) + norm_eps) * gain


def slot_tables(route_block, expert_count, capacity):
    row_count, top_count = route_block.shape
    flat_experts = route_block.reshape(-1)
    one_hot = (flat_experts[:, None] == jnp.arange(expert_count, dtype=jnp.int32)[None, :]).astype(
        jnp.int32
    )
    earlier = jnp.cumsum(one_hot, axis=0) - one_hot
    slot_index = jnp.sum(earlier * one_hot, axis=1)
    flat_slots = slot_index * expert_count + flat_experts
    owner_rows = jnp.full((capacity * expert_count,), row_count, jnp.int32)
    owner_rows = owner_rows.at[flat_slots].set(
        jnp.arange(row_count * top_count, dtype=jnp.int32) // top_count
    )
    return (flat_slots, owner_rows)


def pool_branch(branch_in, pool_weight, group_gain, out_weight, out_gain):
    row_count, width = branch_in.shape
    group_chans = width // len(pool_windows)
    rim = shifted_2(branch_in[row_count - rim_rows :], EP_TP, 1)
    widened = jnp.concatenate([rim, branch_in], axis=0).astype(jnp.float32)
    first_row = (lax.axis_index(EP) * lax.axis_size("tp") + lax.axis_index("tp")) * row_count
    positions = first_row + jnp.arange(row_count, dtype=jnp.int32)
    window = jnp.repeat(jnp.array(pool_windows, jnp.int32), group_chans)
    summed = jnp.zeros((row_count, width), jnp.float32)
    for offset_back in range(rim_rows + 1):
        shifted = widened[rim_rows - offset_back : rim_rows - offset_back + row_count]
        summed = summed + jnp.where(window[None, :] > offset_back, shifted, jnp.float32(0.0))
    counts = jnp.minimum(window[None, :], positions[:, None] + 1).astype(jnp.float32)
    pooled = (summed / counts - widened[rim_rows:]).astype(jnp.bfloat16)
    mixed_parts = []
    for group_index in range(len(pool_windows)):
        lower = group_index * group_chans
        mixed_parts.append(
            jnp.dot(
                pooled[:, lower : lower + group_chans],
                pool_weight[group_index],
                preferred_element_type=jnp.float32,
            )
        )
    group_mix = jnp.concatenate(mixed_parts, axis=1)
    mixed_rows = rms_scale(group_mix, group_gain).astype(jnp.bfloat16)
    projected = jnp.dot(
        mixed_rows, gathered_copies(out_weight, "tp", 1), preferred_element_type=jnp.float32
    )
    return rms_scale(projected, out_gain).astype(jnp.bfloat16)


def expert_hidden(slot_rows, gate_local, up_local):
    gate_pre = jnp.einsum("sed,df->sef", slot_rows, gate_local, preferred_element_type=jnp.float32)
    up_pre = jnp.einsum("sed,df->sef", slot_rows, up_local, preferred_element_type=jnp.float32)
    gate_pre = jnp.minimum(gate_pre, clamp_limit)
    up_pre = jnp.clip(up_pre, -clamp_limit, clamp_limit)
    return ((up_pre + 1.0) * gate_pre * jax.nn.sigmoid(sigmoid_slope * gate_pre)).astype(
        jnp.bfloat16
    )


def send_home(hidden, down_local):
    partial_sum = jnp.einsum("sef,fd->sed", hidden, down_local, preferred_element_type=jnp.float32)
    partial_sum = partial_sum.astype(jnp.bfloat16).astype(jnp.float32)
    summed = sent_and_summed(partial_sum.astype(jnp.bfloat16), "tp", 2).astype(jnp.bfloat16)
    return lax.all_to_all(summed, EP, split_axis=1, concat_axis=1, tiled=True)


def per_device(
    branch_in,
    pool_weight,
    group_gain,
    out_weight,
    out_gain,
    ffn_input,
    ffn_gain,
    routes,
    route_weight,
    gate_weight,
    up_weight,
    down_weight,
):
    mixer_out = pool_branch(branch_in, pool_weight, group_gain, out_weight, out_gain)
    normed_rows = rms_scale(ffn_input.astype(jnp.float32), ffn_gain).astype(jnp.bfloat16)
    row_count, model_width = normed_rows.shape
    top_count = routes.shape[1]
    expert_count = lax.axis_size(EP)
    capacity = 2 * row_count * top_count // expert_count
    flat_slots, owner_rows = slot_tables(routes, expert_count, capacity)
    padded = jnp.concatenate([normed_rows, jnp.zeros((1, model_width), jnp.bfloat16)], axis=0)
    slot_rows = padded[owner_rows].reshape(capacity, expert_count, model_width)
    gate_local = gate_weight[0]
    up_local = up_weight[0]
    down_local = down_weight[0]
    share = capacity // lax.axis_size("tp")
    my_share = lax.dynamic_slice_in_dim(slot_rows, lax.axis_index("tp") * share, share, 0)
    arrived = exchange_by_chip(my_share, ("ep_0", "ep_1"), (1, 0), 1, 1)
    hidden = expert_hidden(lax.all_gather(arrived, "tp", axis=0, tiled=True), gate_local, up_local)
    returned = send_home(hidden, down_local)
    column_count = returned.shape[2]
    picked = returned.reshape(capacity * expert_count, column_count)[flat_slots]
    picked = picked.reshape(row_count, top_count, column_count).astype(jnp.float32)
    expert_out = jnp.sum(picked * route_weight[:, :, None], axis=1).astype(jnp.bfloat16)
    return (mixer_out, expert_out)


def solution(mesh):
    split = Mesh(mesh.devices.reshape(16, 2, mesh.shape["tp"]), ("ep_0", "ep_1", "tp"))
    in_specs = (
        P(EP_TP, None),
        P(),
        P(),
        P(None, "tp"),
        P(),
        P(EP, None),
        P(),
        P(EP, None),
        P(EP, None),
        P(EP, None, "tp"),
        P(EP, None, "tp"),
        P(EP, "tp", None),
    )
    out_specs = (P(EP_TP, None), P(EP, "tp"))
    return jax.shard_map(
        per_device, mesh=split, in_specs=in_specs, out_specs=out_specs, check_vma=False
    )
```

profile of v0, /device:TPU:1, one launch (start us, length us, event | category | flops | bytes accessed | tf_op | source)
XLA Modules:
  0.0 291.9 jit_solution(17089772738966358481)
XLA Ops:
  7.2 0.9 copy.45
  8.1 0.1 eq.29
  8.2 0.1 eq.25
  8.3 0.1 reshape.229
  8.5 1.2 reduce-window.6
  9.6 0.2 slice_reduce_fusion
  9.9 0.1 fusion.60
  10.0 2.4 scatter_custom_fusion
  12.5 1.2 fusion.22
  13.7 1.2 fusion.24
  15.0 6.0 %gather_fusion = bf16[1024,2048]{1,0:T(8,128)(2,1)} fusion(bf16[129,2048]{1,0:T(8,128)(2,1)S(1)} %concatenate.11, s32[1024]{0:T(1024)S(1)} %fusion.78), kind=kCustom, calls=%fused_computation | custom fusion | bytes 8392704 | tf_op jit(solution)/shard_map/gather | solution.py:157
  21.0 1.1 constant_dynamic-slice_fusion
  22.1 0.3 copy.49
  22.4 0.2 copy.50
  22.5 10.4 %all_to_all.25 = bf16[16,2,2,1,2048]{4,0,2,3,1:T(8,128)(2,1)S(1)} all-to-all(bf16[16,2,2,1,2048]{4,0,2,3,1:T(8,128)(2,1)S(1)} %copy.50), channel_id=1, replica_groups=mesh['ep_0'=16,'ep_1'=2,'tp'=16] {'ep_1'}, dimensions={1} | all-to-all | bytes 524288 | tf_op jit(solution)/shard_map/all_to_all | solution.py:56
  33.0 0.3 copy.51
  33.2 23.4 %all_to_all.26 = bf16[16,2,2,1,2048]{4,1,2,3,0:T(2,128)(2,1)S(1)} all-to-all(bf16[16,2,2,1,2048]{4,1,2,3,0:T(2,128)(2,1)S(1)} %copy.51), channel_id=1, replica_groups=mesh['ep_0'=16,'ep_1'=2,'tp'=16] {'ep_0'}, dimensions={0} | all-to-all | bytes 524288 | tf_op jit(solution)/shard_map/all_to_all | solution.py:56
  56.6 0.2 copy.52
  56.9 0.8 copy.53
  57.7 66.4 %all-gather.3.cloned.1.call-done = bf16[32,32,1,2048]{3,1,2,0:T(8,128)(2,1)} async-done(((bf16[2,32,1,2048]{3,1,2,0:T(8,128)(2,1)}), bf16[32,32,1,2048]{3,1,2,0:T(8,128)(2,1)}) %all-gather.3.cloned.1.call-update) | async-done | bytes 4194320 | tf_op jit(solution)/shard_map/all_gather | solution.py:164
  124.1 4.4 %fusion.4 = f32[32,32,256]{2,1,0:T(8,128)} fusion(bf16[32,32,1,2048]{3,1,2,0:T(8,128)(2,1)} %all-gather.3.cloned.1.call-done, bf16[1,2048,256]{2,1,0:T(8,128)(2,1)S(1)} %copy-done.9), kind=kOutput, calls=%fused_computation.11 | convolution fusion | flops 1074003968 | bytes 6291456 | tf_op jit(solution)/shard_map/sed,df->sef/dot_general | solution.py:119
  128.5 8.8 %convert_bitcast_fusion = bf16[32,4,16,8,128]{4,3,2,1,0:T(8,128)(2,1)} fusion(bf16[1,256,2048]{2,1,0:T(8,128)(2,1)S(1)} %copy-done, f32[32,32,256]{2,1,0:T(8,128)} %fusion.4, bf16[32,32,1,2048]{3,1,2,0:T(8,128)(2,1)} %all-gather.3.cloned.1.call-done, bf16[1,2048,256]{2,1,0:T(8,128)(2,1)S(1)} %copy-done.10), kind=kOutput, calls=%fused_computation.8 | convolution fusion | flops 2151940096 | bytes 11534336 | tf_op jit(solution)/shard_map/sef,fd->sed/dot_general | solution.py:129
  137.3 5.2 %copy.62 = bf16[32,4,16,8,128]{4,3,1,0,2:T(8,128)(2,1)} copy(bf16[32,4,16,8,128]{4,3,2,1,0:T(8,128)(2,1)} %convert_bitcast_fusion) | data formatting | bytes 8388608 | tf_op jit(solution)/shard_map/reshape | solution.py:43
  142.5 5.2 %all-to-all-start.3 = ((bf16[16,32,32,128]{3,2,1,0:T(8,128)(2,1)}), bf16[16,32,32,128]{3,2,1,0:T(8,128)(2,1)}, u32[]{:S(2)}, u32[]{:S(2)}) async-start(bf16[16,32,32,128]{3,2,1,0:T(8,128)(2,1)} %bitcast.108), calls=%async_computation.3 | async-start | bytes 8388608 | tf_op jit(solution)/shard_map/all_to_all | solution.py:48
  147.8 3.2 %collective-permute-start = (bf16[15,512]{1,0:T(8,128)(2,1)S(1)}, bf16[15,512]{1,0:T(8,128)(2,1)S(1)}, u32[]{:S(2)}, u32[]{:S(2)}) collective-permute-start(bf16[15,512]{1,0:T(8,128)(2,1)S(1)} %slice.82), channel_id=1, source_target_pairs={{0,1},{1,2},{2,3},{3,4},{4,5},{5,6},{6,7},{7,8},{8,9},{9,10},{10,1... | collective-permute-start | bytes 46088 | tf_op jit(solution)/shard_map/ppermute | solution.py:21
  151.0 0.1 copy.44
  151.2 0.1 bitcast_compare_fusion.15
  151.3 58.6 %all-to-all-done.3 = bf16[16,32,32,128]{3,2,1,0:T(8,128)(2,1)} async-done(((bf16[16,32,32,128]{3,2,1,0:T(8,128)(2,1)}), bf16[16,32,32,128]{3,2,1,0:T(8,128)(2,1)}, u32[]{:S(2)}, u32[]{:S(2)}) %all-to-all-start.3) | async-done | bytes 4194336 | tf_op jit(solution)/shard_map/all_to_all | solution.py:48
  209.9 1.5 broadcast_in_dim.147
  211.4 4.2 %all-to-all-start = ((bf16[16,512,128]{1,2,0:T(8,128)(2,1)}), bf16[16,512,128]{1,2,0:T(8,128)(2,1)S(1)}, u32[]{:S(2)}, u32[]{:S(2)}) async-start(bf16[16,512,128]{1,2,0:T(8,128)(2,1)} %broadcast_in_dim.147), calls=%async_computation | async-start | bytes 4194304 | tf_op jit(solution)/shard_map/all_to_all | solution.py:32
  215.6 0.7 copy.57
  216.5 1.1 fusion.53
  217.6 0.2 fusion.61
  217.8 0.2 fusion.63
  218.1 0.2 fusion.65
  218.3 0.2 fusion.67
  218.5 0.6 copy-done.1
  219.1 0.1 multiply_reduce_fusion.1
  219.2 3.6 %reduce_sum.61 = bf16[32,32,128]{2,1,0:T(8,128)(2,1)} reduce(bf16[16,32,32,128]{3,2,1,0:T(8,128)(2,1)} %all-to-all-done.3, bf16[]{:T(256)} %constant.99.clone.1), dimensions={0}, to_apply=%region_7.8 | reduce | flops 1966080 | bytes 4456450 | tf_op jit(solution)/shard_map/reduce_sum | solution.py:49
  222.8 1.7 copy.55
  224.5 17.7 %all-to-all-done = bf16[16,512,128]{1,2,0:T(8,128)(2,1)S(1)} async-done(((bf16[16,512,128]{1,2,0:T(8,128)(2,1)}), bf16[16,512,128]{1,2,0:T(8,128)(2,1)S(1)}, u32[]{:S(2)}, u32[]{:S(2)}) %all-to-all-start) | async-done | bytes 2097184 | tf_op jit(solution)/shard_map/all_to_all | solution.py:32
  242.2 17.3 %all-to-all-start.4 = ((bf16[32,32,128]{2,0,1:T(8,128)(2,1)}), bf16[32,32,128]{2,0,1:T(8,128)(2,1)}, u32[]{:S(2)}, u32[]{:S(2)}) async-start(bf16[32,32,128]{2,0,1:T(8,128)(2,1)} %copy.55), calls=%async_computation.4 | async-start | bytes 524288 | tf_op jit(solution)/shard_map/all_to_all | solution.py:132
  259.5 1.9 multiply_reduce_fusion
  261.4 1.2 multiply_convert_fusion
  262.6 19.2 %all-to-all-done.4 = bf16[32,32,128]{2,0,1:T(8,128)(2,1)} async-done(((bf16[32,32,128]{2,0,1:T(8,128)(2,1)}), bf16[32,32,128]{2,0,1:T(8,128)(2,1)}, u32[]{:S(2)}, u32[]{:S(2)}) %all-to-all-start.4) | async-done | bytes 262176 | tf_op jit(solution)/shard_map/all_to_all | solution.py:132
  281.8 1.1 copy.56
  282.9 1.3 gather_fusion.1
  284.2 0.9 fusion.55
  (40 shorter events, 0.4 us)
Async XLA Ops:
  7.2 121.3 %copy-start = (bf16[1,256,2048]{2,1,0:T(8,128)(2,1)S(1)}, bf16[1,256,2048]{2,1,0:T(8,128)(2,1)}, u32[]{:S(2)}) copy-start(bf16[1,256,2048]{2,1,0:T(8,128)(2,1)} %param.24) | copy-start | bytes 3145732
  7.2 116.9 %all-gather.3.cloned.1.call-start = ((), (), s32[]{:S(2)}) async-start(), calls=%async_computation.5 | async-start | bytes 4456448 | tf_op jit(solution)/shard_map/all_gather | solution.py:164
  21.0 103.0 %copy-start.9 = (bf16[1,2048,256]{2,1,0:T(8,128)(2,1)S(1)}, bf16[1,2048,256]{2,1,0:T(8,128)(2,1)}, u32[]{:S(2)}) copy-start(bf16[1,2048,256]{2,1,0:T(8,128)(2,1)} %param.22) | copy-start | bytes 3145732
  57.7 70.8 %copy-start.10 = (bf16[1,2048,256]{2,1,0:T(8,128)(2,1)S(1)}, bf16[1,2048,256]{2,1,0:T(8,128)(2,1)}, u32[]{:S(2)}) copy-start(bf16[1,2048,256]{2,1,0:T(8,128)(2,1)} %param.23) | copy-start | bytes 3145732
  142.5 5.2 %copy-start.2 = (bf16[256,512]{1,0:T(8,128)(2,1)S(1)}, bf16[256,512]{1,0:T(8,128)(2,1)}, u32[]{:S(2)}) copy-start(bf16[256,512]{1,0:T(8,128)(2,1)} %param.13) | copy-start | bytes 786436
  142.5 8.4 %copy-start.5 = (bf16[512,128]{1,0:T(8,128)(2,1)S(1)}, bf16[512,128]{1,0:T(8,128)(2,1)}, u32[]{:S(2)}) copy-start(bf16[512,128]{1,0:T(8,128)(2,1)} %param.16) | copy-start | bytes 393220
  142.5 8.6 %copy-start.8 = (s32[4]{0:T(128)S(1)}, s32[4]{0:T(128)}, u32[]{:S(2)}) copy-start(s32[4]{0:T(128)} %constant.108.clone) | copy-start | bytes 52
  142.5 67.3 %all-to-all-start.3 = ((bf16[16,32,32,128]{3,2,1,0:T(8,128)(2,1)}), bf16[16,32,32,128]{3,2,1,0:T(8,128)(2,1)}, u32[]{:S(2)}, u32[]{:S(2)}) async-start(bf16[16,32,32,128]{3,2,1,0:T(8,128)(2,1)} %bitcast.108), calls=%async_computation.3 | async-start | bytes 8388608 | tf_op jit(solution)/shard_map/all_to_all | solution.py:48
  147.7 67.9 %copy-start.7 = (f32[128,4]{0,1:T(4,128)S(1)}, f32[128,4]{0,1:T(4,128)}, u32[]{:S(2)}) copy-start(f32[128,4]{0,1:T(4,128)} %param.21) | copy-start | bytes 6148
  147.8 68.6 %collective-permute-start = (bf16[15,512]{1,0:T(8,128)(2,1)S(1)}, bf16[15,512]{1,0:T(8,128)(2,1)S(1)}, u32[]{:S(2)}, u32[]{:S(2)}) collective-permute-start(bf16[15,512]{1,0:T(8,128)(2,1)S(1)} %slice.82), channel_id=1, source_target_pairs={{0,1},{1,2},{2,3},{3,4},{4,5},{5,6},{6,7},{7,8},{8,9},{9,10},{10,1... | collective-permute-start | bytes 46088 | tf_op jit(solution)/shard_map/ppermute | solution.py:21
  211.4 30.8 %all-to-all-start = ((bf16[16,512,128]{1,2,0:T(8,128)(2,1)}), bf16[16,512,128]{1,2,0:T(8,128)(2,1)S(1)}, u32[]{:S(2)}, u32[]{:S(2)}) async-start(bf16[16,512,128]{1,2,0:T(8,128)(2,1)} %broadcast_in_dim.147), calls=%async_computation | async-start | bytes 4194304 | tf_op jit(solution)/shard_map/all_to_all | solution.py:32
  216.4 1.2 copy-start.4
  218.5 0.6 copy-start.1
  219.2 42.2 %copy-start.6 = (f32[2048]{0:T(1024)S(1)}, f32[2048]{0:T(1024)}, u32[]{:S(2)}) copy-start(f32[2048]{0:T(1024)} %param.17) | copy-start | bytes 24580
  242.2 39.6 %all-to-all-start.4 = ((bf16[32,32,128]{2,0,1:T(8,128)(2,1)}), bf16[32,32,128]{2,0,1:T(8,128)(2,1)}, u32[]{:S(2)}, u32[]{:S(2)}) async-start(bf16[32,32,128]{2,0,1:T(8,128)(2,1)} %copy.55), calls=%async_computation.4 | async-start | bytes 524288 | tf_op jit(solution)/shard_map/all_to_all | solution.py:132
  261.4 22.8 %copy-start.3 = (f32[128,4]{1,0:T(8,128)S(1)}, f32[128,4]{1,0:T(8,128)}, u32[]{:S(2)}) copy-start(f32[128,4]{1,0:T(8,128)} %copy.57) | copy-start | bytes 6148
Sparse Core Ops, SparseCore 0:
  57.8 66.2 all-gather.2
where the time goes:
time: 293 us; the launch traced here: 292 us
  waiting for transfers between devices  162 us (55%)
  blocking collectives  33.8 us (12%)
  starting transfers between devices  29.9 us (10%)
  local copies, waits for them, and re-layouts  25.2 us (9%)
  matrix products  15.9 us (5%)
  between operations  14.4 us (5%)
  other arithmetic  10.9 us (4%)
    all_gather x1, waiting for transfers between devices, per_device(): lax.all_gather(arrived, 'tp', axis=0, tiled=True)  66.4 us
    all_to_all x1, waiting for transfers between devices, sent_and_summed(): lax.all_to_all(in_blocks(shard, dim, devices), axis, 0, 0, tiled=True)  58.6 us
    all_to_all x2, blocking collectives, exchange_in_order(): filled = lax.all_to_all(filled, axes[k], k, k, tiled=True)  33.8 us
    all_to_all x1, waiting for transfers between devices, send_home(): return lax.all_to_all(summed, EP, split_axis=1, concat_axis=1, tiled=True)  19.2 us
    all_to_all x1, waiting for transfers between devices, from_everyone(): lax.all_to_all(jnp.broadcast_to(shard[None], (devices, *shard.shape)), ax...  17.7 us
    all_to_all x1, starting transfers between devices, send_home(): return lax.all_to_all(summed, EP, split_axis=1, concat_axis=1, tiled=True)  17.3 us
    dot_general x1, matrix products, send_home(): jnp.einsum('sef,fd->sed', hidden, down_local, preferred_element_type=jnp....  8.8 us
    gather x1, local copies, waits for them, and re-layouts, per_device(): slot_rows = padded[owner_rows].reshape(capacity, expert_count, model_width)  6.02 us
  transfers between devices with their start and end apart: 5, of which 4 were waited for; matrix products, arithmetic and copies ran while one was open for 4% of the time, Pallas kernels for 0%

commit v1 on v0

v1 whole, which is shorter than its diff:
```python
import functools

import jax
import jax.numpy as jnp
from jax import lax
from jax.experimental import pallas as pl
from jax.experimental.pallas import tpu as pltpu
from jax.sharding import Mesh
from jax.sharding import PartitionSpec as P

MESH = pl.DeviceIdType.MESH
AXES = ("z", "c", "y", "x")
EP = ("z", "c")
TP = ("y", "x")

pool_windows = (2, 4, 8, 16)
norm_eps = 1e-06
clamp_limit = 7.0
sigmoid_slope = 1.702

BF = jnp.bfloat16
F32 = jnp.float32

NZ, NC, NY, NX = 16, 2, 4, 4
CAP = 32
LANE = 128
CHUNKS = 4
RIM = 16


def dot(a, b):
    return jnp.dot(a, b, preferred_element_type=F32)


def kernel(
    branch,
    pool_w,
    group_gain,
    out_w,
    out_gain,
    ffn_in,
    ffn_gain,
    routes_t,
    weight_t,
    gate_w,
    up_w,
    down_w,
    mixer_out,
    expert_out,
    full,
    other_w,
    gate_up,
    down_p,
    ext,
    mixed,
    proj,
    mixer,
    tokens,
    hot,
    picked,
    part,
    rx1,
    rx2,
    sum_x,
    ry1,
    ry2,
    home,
    result,
    ag_s,
    ag_r,
    rs_s,
    rs_r,
    z_s,
    z_r,
    back_s,
    back_r,
    own_s,
    swap_s,
    rim_s,
    load_s,
):
    z, c = lax.axis_index("z"), lax.axis_index("c")
    y, x = lax.axis_index("y"), lax.axis_index("x")
    ep = z * NC + c
    tp = y * NX + x
    rows_a = branch.shape[0]
    rows_b = ffn_in.shape[0]
    model = ffn_in.shape[1]
    hid = gate_w.shape[2]
    width = branch.shape[1]
    slots = NZ * NC * CAP
    crow = slots // CHUNKS
    half = crow // 2
    per = NZ // CHUNKS
    wide = NY * LANE

    spot = (ep * NY + y) * NX + x
    total = NZ * NC * NY * NX

    def place(index):
        return (index // (NC * NY * NX), (index // (NY * NX)) % NC, (index // NX) % NY, index % NX)

    after = place((spot + 1) % total)
    before = place((spot + total - 1) % total)
    x_to = ((z, c, y, (x + 1) % NX), (z, c, y, (x + NX - 1) % NX))
    y_to = ((z, c, (y + 1) % NY, x), (z, c, (y + NY - 1) % NY, x))
    partner = (z, 1 - c, y, x)

    def step_z(i):
        return (z + NZ + ((i + 1) // 2) * (2 * (i % 2) - 1)) % NZ

    loads = {}

    def load(name, src, dst, slot):
        copy = pltpu.make_async_copy(src, dst, load_s.at[slot])
        copy.start()
        loads[name] = copy

    load("tokens", ffn_in, tokens, 0)
    load("branch", branch, ext.at[pl.ds(RIM, rows_a)], 1)
    own_cols = pl.ds(pl.multiple_of(tp * LANE, LANE), LANE)
    load("out_w", out_w.at[pl.ds(pl.multiple_of(c * crow, crow), crow)], full.at[pl.ds(0, crow), own_cols], 2)
    load("gate", gate_w.at[0], gate_up.at[:, pl.ds(0, hid)], 3)
    load("up", up_w.at[0], gate_up.at[:, pl.ds(hid, hid)], 4)
    for a in range(NY):
        for b in range(NX):
            load(
                ("down", a, b),
                down_w.at[0, :, pl.ds((a * NX + b) * LANE, LANE)],
                down_p.at[:, pl.ds((b * NY + a) * LANE, LANE)],
                5 + a * NX + b,
            )

    barrier = pltpu.get_barrier_semaphore()

    def greet(i, carry):
        zz = step_z(i)
        for cc in range(NC):
            pl.semaphore_signal(barrier, inc=1, device_id=(zz, cc, y, x), device_id_type=MESH)
        return carry

    for peer in (*x_to, *y_to, after, before, partner):
        pl.semaphore_signal(barrier, inc=1, device_id=peer, device_id_type=MESH)
    lax.fori_loop(1, NZ, greet, 0)

    loads["tokens"].wait()
    acc = jnp.zeros((rows_b, LANE), F32)
    for k in range(model // LANE):
        v = tokens[:, k * LANE : (k + 1) * LANE].astype(F32)
        acc = acc + v * v
    scale = lax.rsqrt(jnp.sum(acc, axis=1, keepdims=True) * (1.0 / model) + norm_eps)
    normed = (tokens[:, own_cols].astype(F32) * scale * ffn_gain[:, own_cols]).astype(BF)

    experts = NZ * NC
    ids = lax.broadcasted_iota(jnp.int32, (experts, rows_b), 0)
    named = jnp.zeros((experts, rows_b), F32)
    weight = jnp.zeros((experts, rows_b), F32)
    for k in range(routes_t.shape[0]):
        hit = ids == routes_t[k : k + 1, :]
        named = named + jnp.where(hit, 1.0, 0.0)
        weight = weight + jnp.where(hit, weight_t[k : k + 1, :], 0.0)
    earlier = jnp.where(
        lax.broadcasted_iota(jnp.int32, (rows_b, rows_b), 0)
        < lax.broadcasted_iota(jnp.int32, (rows_b, rows_b), 1),
        1.0,
        0.0,
    ).astype(BF)
    place_of = jnp.where(named > 0.5, dot(named.astype(BF), earlier), -1.0)
    slot_ids = lax.broadcasted_iota(jnp.int32, (CAP, rows_b), 0).astype(F32)
    for e in range(experts):
        hot[e * CAP : (e + 1) * CAP, :] = jnp.where(slot_ids == place_of[e : e + 1, :], 1.0, 0.0).astype(BF)
    picked[...] = dot(hot[...], normed).astype(BF)

    pl.semaphore_wait(barrier, 2 * (NZ - 1) + 7)

    loads["branch"].wait()
    rim = pltpu.make_async_remote_copy(
        ext.at[pl.ds(rows_a, RIM)],
        ext.at[pl.ds(0, RIM)],
        send_sem=rim_s.at[0],
        recv_sem=rim_s.at[1],
        device_id=after,
        device_id_type=MESH,
    )
    rim.start()

    def base(g):
        return g * crow

    sends = [rim]

    def push(src, dst, sems, index, peer):
        send, recv = sems
        copy = pltpu.make_async_remote_copy(
            src,
            dst,
            send_sem=send.at[index],
            recv_sem=recv.at[index],
            device_id=peer,
            device_id_type=MESH,
        )
        copy.start()
        sends.append(copy)
        return copy

    gather = {}

    def cols_x(which):
        return pl.ds(pl.multiple_of((y * NX + which % NX) * LANE, LANE), LANE)

    def cols_y(which):
        return pl.ds(pl.multiple_of((which % NY) * wide, wide), wide)

    def ag1(g):
        ref = full.at[pl.ds(base(g), crow), cols_x(x)]
        gather[g, 0] = [push(ref, ref, (ag_s, ag_r), g * 8 + d, x_to[d]) for d in range(2)]

    def ag2(g):
        out = []
        for d in range(2):
            gather[g, 0][d].wait_recv()
            ref = full.at[pl.ds(base(g) + d * half, half), cols_x(x + NX - 1 + 2 * d)]
            out.append(push(ref, ref, (ag_s, ag_r), g * 8 + 2 + d, x_to[d]))
        gather[g, 1] = out

    def ag3(g):
        for d in range(2):
            gather[g, 1][d].wait_recv()
        ref = full.at[pl.ds(base(g), crow), cols_y(y)]
        gather[g, 2] = [push(ref, ref, (ag_s, ag_r), g * 8 + 4 + d, y_to[d]) for d in range(2)]

    def ag4(g):
        out = []
        for d in range(2):
            gather[g, 2][d].wait_recv()
            ref = full.at[pl.ds(base(g) + d * half, half), cols_y(y + NY - 1 + 2 * d)]
            out.append(push(ref, ref, (ag_s, ag_r), g * 8 + 6 + d, y_to[d]))
        gather[g, 3] = out

    def ag5(g):
        for d in range(2):
            gather[g, 3][d].wait_recv()

    own_pick = pltpu.make_async_copy(
        picked.at[pl.ds(pl.multiple_of(ep * CAP, CAP), CAP)],
        full.at[pl.ds(pl.multiple_of(crow + c * CAP, CAP), CAP), own_cols],
        own_s.at[0],
    )

    def dispatch(i, zz, cc, seat):
        row = pl.multiple_of(crow + (seat * NC + c) * CAP, CAP)
        return pltpu.make_async_remote_copy(
            picked.at[pl.ds(pl.multiple_of((zz * NC + cc) * CAP, CAP), CAP)],
            full.at[pl.ds(row, CAP), own_cols],
            send_sem=z_s.at[0],
            recv_sem=z_r.at[seat // per],
            device_id=(zz, cc, y, x),
            device_id_type=MESH,
        )

    def dispatch_all(i, carry):
        zz = step_z(i)
        seat = jnp.minimum(i + 2 * (i % 2) - 1, NZ - 1)
        for cc in range(NC):
            dispatch(i, zz, cc, seat).start()
        return carry

    loads["out_w"].wait()
    own_pick.start()
    dispatch(0, z, 1 - c, 0).start()
    ag1(0)
    lax.fori_loop(1, NZ, dispatch_all, 0)

    def arrived(g):
        count = crow - CAP if g == 1 else crow
        ref = full.at[pl.ds(base(g), count), own_cols]
        pltpu.make_async_copy(ref, ref, z_r.at[g - 1]).wait()
        if g == 1:
            own_pick.wait()

    def pool_mix():
        rim.wait_recv()
        reach = rows_a + RIM
        row = lax.broadcasted_iota(jnp.int32, (rows_a, reach), 0) + RIM
        col = lax.broadcasted_iota(jnp.int32, (rows_a, reach), 1)
        first = jnp.where(spot == 0, RIM, 0)
        age = jnp.where(col < first, reach, row - col)
        position = spot * rows_a + lax.broadcasted_iota(jnp.int32, (rows_a, LANE), 0)
        parts = []
        acc = jnp.zeros((rows_a, LANE), F32)
        for k, window in enumerate(pool_windows):
            cols = slice(k * LANE, (k + 1) * LANE)
            band = jnp.where((age >= 0) & (age < window), 1.0, 0.0).astype(BF)
            summed = dot(band, ext[:, cols])
            count = jnp.minimum(position + 1, window).astype(F32)
            pooled = (summed / count - ext[RIM:, cols].astype(F32)).astype(BF)
            mix = dot(pooled, pool_w[k])
            parts.append(mix)
            acc = acc + mix * mix
        scale = lax.rsqrt(jnp.sum(acc, axis=1, keepdims=True) * (1.0 / width) + norm_eps)
        for k, mix in enumerate(parts):
            cols = slice(k * LANE, (k + 1) * LANE)
            mixed[:, cols] = (mix * scale * group_gain[:, cols]).astype(BF)

    swap = pltpu.make_async_remote_copy(
        full.at[pl.ds(0, crow)],
        other_w,
        send_sem=swap_s.at[0],
        recv_sem=swap_s.at[1],
        device_id=partner,
        device_id_type=MESH,
    )

    def swap_halves():
        swap.start()
        sends.append(swap)

    store = pltpu.make_async_copy(mixer, mixer_out, load_s.at[21])

    def pool_out():
        swap.wait_recv()
        mine = mixed[:, pl.ds(pl.multiple_of(c * crow, crow), crow)]
        theirs = mixed[:, pl.ds(pl.multiple_of((1 - c) * crow, crow), crow)]
        acc = jnp.zeros((rows_a, LANE), F32)
        tile = 256
        for n in range(model // tile):
            cols = slice(n * tile, (n + 1) * tile)
            v = dot(mine, full[0:crow, cols]) + dot(theirs, other_w[:, cols])
            proj[:, cols] = v
            for k in range(tile // LANE):
                w = v[:, k * LANE : (k + 1) * LANE]
                acc = acc + w * w
        scale = lax.rsqrt(jnp.sum(acc, axis=1, keepdims=True) * (1.0 / model) + norm_eps)
        for n in range(model // tile):
            cols = slice(n * tile, (n + 1) * tile)
            mixer[:, cols] = (proj[:, cols] * scale * out_gain[:, cols]).astype(BF)
        store.start()

    reduce = {}

    def block(which, count):
        return pl.ds(pl.multiple_of((which % NX) * count, count), count)

    def compute(g):
        ag5(g)
        if g == 1:
            loads["gate"].wait()
            loads["up"].wait()
            for a in range(NY):
                for b in range(NX):
                    loads["down", a, b].wait()
        both = dot(full[base(g) : base(g) + crow, :], gate_up[...])
        gate = jnp.minimum(both[:, :hid], clamp_limit)
        up = jnp.clip(both[:, hid:], -clamp_limit, clamp_limit)
        hidden = ((up + 1.0) * gate * jax.nn.sigmoid(sigmoid_slope * gate)).astype(BF)
        r = base(g - 1)
        for k in range(NX):
            cols = block(x + 2 + k, wide)
            part[r : r + crow, cols] = dot(hidden, down_p[:, cols]).astype(BF)
            if k == 0:
                reduce[g, 0] = [
                    push(
                        part.at[pl.ds(r + d * half, half), cols],
                        rx1.at[pl.ds(r + d * half, half)],
                        (rs_s, rs_r),
                        (g - 1) * 8 + d,
                        x_to[d],
                    )
                    for d in range(2)
                ]

    def add(*values):
        out = values[0].astype(F32)
        for v in values[1:]:
            out = out + v.astype(F32)
        return out.astype(BF)

    def rs2(g):
        r = base(g - 1)
        out = []
        for d in range(2):
            reduce[g, 0][d].wait_recv()
            cols = block(x + 1 + 2 * d, wide)
            rows = slice(r + d * half, r + d * half + half)
            part[rows, cols] = add(part[rows, cols], rx1[rows, :])
            out.append(
                push(
                    part.at[pl.ds(r, crow), cols],
                    rx2.at[pl.ds(r, crow), pl.ds(d * wide, wide)],
                    (rs_s, rs_r),
                    (g - 1) * 8 + 2 + d,
                    x_to[d],
                )
            )
        reduce[g, 1] = out

    def rs3(g):
        r = base(g - 1)
        for d in range(2):
            reduce[g, 1][d].wait_recv()
        rows = slice(r, r + crow)
        sum_x[rows, :] = add(part[rows, block(x, wide)], rx2[rows, :wide], rx2[rows, wide:])
        cols = block(y + 2, LANE)
        reduce[g, 2] = [
            push(
                sum_x.at[pl.ds(r + d * half, half), cols],
                ry1.at[pl.ds(r + d * half, half)],
                (rs_s, rs_r),
                (g - 1) * 8 + 4 + d,
                y_to[d],
            )
            for d in range(2)
        ]

    def rs4(g):
        r = base(g - 1)
        out = []
        for d in range(2):
            reduce[g, 2][d].wait_recv()
            cols = block(y + 1 + 2 * d, LANE)
            rows = slice(r + d * half, r + d * half + half)
            sum_x[rows, cols] = add(sum_x[rows, cols], ry1[rows, :])
            out.append(
                push(
                    sum_x.at[pl.ds(r, crow), cols],
                    ry2.at[pl.ds(r, crow), pl.ds(d * LANE, LANE)],
                    (rs_s, rs_r),
                    (g - 1) * 8 + 6 + d,
                    y_to[d],
                )
            )
        reduce[g, 3] = out

    own_rows = pl.ds(pl.multiple_of(ep * CAP, CAP), CAP)
    own_back = pltpu.make_async_copy(
        home.at[pl.ds(pl.multiple_of(c * CAP, CAP), CAP)], result.at[own_rows], own_s.at[1]
    )

    def give_back(i, cc):
        return pltpu.make_async_remote_copy(
            home.at[pl.ds(pl.multiple_of((i * NC + cc) * CAP, CAP), CAP)],
            result.at[own_rows],
            send_sem=back_s.at[0],
            recv_sem=back_r.at[0],
            device_id=(step_z(i), cc, y, x),
            device_id_type=MESH,
        )

    def rs5(g):
        r = base(g - 1)
        for d in range(2):
            reduce[g, 3][d].wait_recv()
        rows = slice(r, r + crow)
        home[rows, :] = add(sum_x[rows, block(y, LANE)], ry2[rows, :LANE], ry2[rows, LANE:])
        low = (g - 1) * per
        if g == 1:
            own_back.start()
            give_back(0, 1 - c).start()
            low = 1

        def one(i, carry):
            for cc in range(NC):
                give_back(i, cc).start()
            return carry

        lax.fori_loop(low, g * per, one, 0)

    stages = (ag1, ag2, ag3, ag4, compute, rs2, rs3, rs4, rs5)
    for tick in range(len(stages) + CHUNKS):
        for g in range(CHUNKS + 1):
            k = tick - g
            if g == 0:
                if 1 <= k < 4:
                    stages[k](0)
                elif k == 4:
                    ag5(0)
                    swap_halves()
            elif 0 <= k < len(stages):
                if k == 0:
                    if g == 1:
                        pool_mix()
                    arrived(g)
                stages[k](g)
        if tick == 7:
            pool_out()

    own_back.wait()
    ref = result.at[pl.ds(0, slots - CAP)]
    pltpu.make_async_copy(ref, ref, back_r.at[0]).wait()
    ref = picked.at[pl.ds(0, slots - CAP)]
    pltpu.make_async_copy(ref, ref, z_s.at[0]).wait()
    w_hi = weight.astype(BF).astype(F32)
    w_lo = weight - w_hi
    acc = jnp.zeros((rows_b, LANE), F32)
    for e in range(experts):
        rows = slice(e * CAP, (e + 1) * CAP)
        h = hot[rows, :].astype(F32)
        picked[rows, :] = (h * w_hi[e : e + 1, :]).astype(BF)
        hot[rows, :] = (h * w_lo[e : e + 1, :]).astype(BF)
    over = (((0,), (0,)), ((), ()))
    value = lax.dot_general(picked[...], result[...], over, preferred_element_type=F32)
    value = value + lax.dot_general(hot[...], result[...], over, preferred_element_type=F32)
    expert_out[...] = value.astype(BF)

    store.wait()
    for copy in sends:
        copy.wait_send()
    ref = home.at[pl.ds(0, slots - CAP)]
    pltpu.make_async_copy(ref, ref, back_s.at[0]).wait()


def per_device(
    branch_in,
    pool_weight,
    group_gain,
    out_weight,
    out_gain,
    ffn_input,
    ffn_gain,
    routes,
    route_weight,
    gate_weight,
    up_weight,
    down_weight,
):
    rows_a, width = branch_in.shape
    rows_b, model = ffn_input.shape
    hid = gate_weight.shape[2]
    slots = NZ * NC * CAP
    crow = slots // CHUNKS
    half = crow // 2
    wide = NY * LANE
    any_ = pl.BlockSpec(memory_space=pl.ANY)
    vmem = pl.BlockSpec(memory_space=pltpu.VMEM)
    dma = pltpu.SemaphoreType.DMA
    return pl.pallas_call(
        kernel,
        name="mixer_and_experts",
        out_shape=(
            jax.ShapeDtypeStruct((rows_a, model), BF),
            jax.ShapeDtypeStruct((rows_b, LANE), BF),
        ),
        in_specs=[any_, vmem, vmem, any_, vmem, any_, vmem, vmem, vmem, any_, any_, any_],
        out_specs=(any_, vmem),
        scratch_shapes=[
            pltpu.VMEM((crow + slots, model), BF),
            pltpu.VMEM((crow, model), BF),
            pltpu.VMEM((model, 2 * hid), BF),
            pltpu.VMEM((hid, model), BF),
            pltpu.VMEM((rows_a + RIM, width), BF),
            pltpu.VMEM((rows_a, width), BF),
            pltpu.VMEM((rows_a, model), F32),
            pltpu.VMEM((rows_a, model), BF),
            pltpu.VMEM((rows_b, model), BF),
            pltpu.VMEM((slots, rows_b), BF),
            pltpu.VMEM((slots, LANE), BF),
            pltpu.VMEM((slots, model), BF),
            pltpu.VMEM((slots, wide), BF),
            pltpu.VMEM((slots, 2 * wide), BF),
            pltpu.VMEM((slots, wide), BF),
            pltpu.VMEM((slots, LANE), BF),
            pltpu.VMEM((slots, 2 * LANE), BF),
            pltpu.VMEM((slots, LANE), BF),
            pltpu.VMEM((slots, LANE), BF),
            dma(((CHUNKS + 1) * 8,)),
            dma(((CHUNKS + 1) * 8,)),
            dma((CHUNKS * 8,)),
            dma((CHUNKS * 8,)),
            dma((1,)),
            dma((CHUNKS,)),
            dma((1,)),
            dma((1,)),
            dma((2,)),
            dma((2,)),
            dma((2,)),
            dma((22,)),
        ],
        compiler_params=pltpu.CompilerParams(collective_id=0, has_side_effects=True),
    )(
        branch_in,
        pool_weight,
        group_gain[None],
        out_weight,
        out_gain[None],
        ffn_input,
        ffn_gain[None],
        routes.T,
        route_weight.T,
        gate_weight,
        up_weight,
        down_weight,
    )


def solution(mesh):
    split = Mesh(mesh.devices.reshape(NZ, NC, NY, NX), AXES)
    in_specs = (
        P(AXES, None),
        P(),
        P(),
        P(None, TP),
        P(),
        P(EP, None),
        P(),
        P(EP, None),
        P(EP, None),
        P(EP, None, TP),
        P(EP, None, TP),
        P(EP, TP, None),
    )
    out_specs = (P(AXES, None), P(EP, TP))
    return jax.shard_map(
        per_device, mesh=split, in_specs=in_specs, out_specs=out_specs, check_vma=False
    )
```

time: 293 us -> 109 us (0.37)
  waiting for transfers between devices: 162 us -> 0 us
  Pallas kernels: 0 us -> 105 us
  blocking collectives: 33.8 us -> 0 us
  starting transfers between devices: 29.9 us -> 0 us
  local copies, waits for them, and re-layouts: 25.2 us -> 2.93 us
  matrix products: 15.9 us -> 0 us
  between operations: 14.4 us -> 0.65 us
  other arithmetic: 10.9 us -> 0 us
    pallas_call x0 -> x1, Pallas kernels: none -> 105 us  [per_device(): pl.pallas_call(kernel, name='mixer_and_experts', out_shape=(jax.ShapeDtyp...]
    all_to_all x3 -> x0, waiting for transfers between devices: 95.5 us -> none  [the longest x1 58.6 us: sent_and_summed(): lax.all_to_all(in_blocks(shard, dim, devices), axis, 0, 0, tiled=True)]
    all_gather x1 -> x0, waiting for transfers between devices: 66.4 us -> none  [per_device(): lax.all_gather(arrived, 'tp', axis=0, tiled=True)]
    all_to_all x2 -> x0, blocking collectives: 33.8 us -> none  [exchange_in_order(): filled = lax.all_to_all(filled, axes[k], k, k, tiled=True)]
    all_to_all x3 -> x0, starting transfers between devices: 26.6 us -> none  [the longest x1 17.3 us: send_home(): return lax.all_to_all(summed, EP, split_axis=1, concat_axis=1, tiled=True)]
    dot_general x7 -> x0, matrix products: 15.9 us -> none  [the longest x1 8.8 us: send_home(): jnp.einsum('sef,fd->sed', hidden, down_local, preferred_element_type=jnp....]
    gather x2 -> x0, local copies, waits for them, and re-layouts: 7.36 us -> none  [the longest x1 6.02 us: per_device(): slot_rows = padded[owner_rows].reshape(capacity, expert_count, model_width)]
    reduce_sum x5 -> x0, other arithmetic: 5.85 us -> none  [the longest x1 3.55 us: sent_and_summed(): return jnp.sum(parts.astype(jnp.float32), axis=0)]
  transfers between devices with their start and end apart: 5 -> 0, of which waited for: 4 -> 0; matrix products, arithmetic and copies ran while one was open for 4% -> 0% of each run, Pallas kernels for 0% -> 0%
where the time goes in v1:
time: 109 us
  Pallas kernels  105 us (96%)
  local copies, waits for them, and re-layouts  2.93 us (3%)
    pallas_call x1, Pallas kernels, per_device(): pl.pallas_call(kernel, name='mixer_and_experts', out_shape=(jax.ShapeDtyp...  105 us
    unnamed x4, local copies, waits for them, and re-layouts  2.93 us

profile of v1, /device:TPU:1, one launch (start us, length us, event | category | flops | bytes accessed | tf_op | source)
XLA Modules:
  0.0 108.8 jit_solution(17800921638254432499)
XLA Ops:
  0.6 105.2 %mixer_and_experts.1 = (bf16[256,2048]{1,0:T(8,128)(2,1)}, bf16[128,128]{1,0:T(8,128)(2,1)}) custom-call(bf16[256,512]{1,0:T(8,128)(2,1)} %branch.1, bf16[4,128,128]{2,1,0:T(8,128)(2,1)} %pool_w.1, f32[1,512]{1,0:T(1,128)} %bitcast.7, bf16[512,128]{1,0:T(8,128)(2,1)} %out_w.1, f32[1,2048]{1,0:T(1,128)} %bitcast.5, bf16[128,2048]{1,0:T(8,128)(2,1)} %ffn_in.1, ...), custom_call_target="tpu_custom_call" | custom-call | tf_op jit(solution)/shard_map/mixer_and_experts/pallas_call | solution.py:536
  105.9 0.0 copy-start
  105.9 2.3 %copy.16 = bf16[256,2048]{1,0:T(8,128)(2,1)} copy(bf16[256,2048]{1,0:T(8,128)(2,1)} %get-tuple-element.4) | data formatting | bytes 2097152
  108.2 0.0 copy-done
  108.2 0.6 copy.17
Async XLA Ops:
  105.9 2.3 %copy-start = (bf16[128,128]{1,0:T(8,128)(2,1)S(1)}, bf16[128,128]{1,0:T(8,128)(2,1)}, u32[]{:S(2)}) copy-start(bf16[128,128]{1,0:T(8,128)(2,1)} %get-tuple-element.5) | copy-start | bytes 98308

commit v2 on v1

v2 whole, which is shorter than its diff:
```python
import functools

import jax
import jax.numpy as jnp
from jax import lax
from jax.experimental import pallas as pl
from jax.experimental.pallas import tpu as pltpu
from jax.sharding import Mesh
from jax.sharding import PartitionSpec as P

MESH = pl.DeviceIdType.MESH
AXES = ("z", "c", "y", "x")
EP = ("z", "c")
TP = ("y", "x")

pool_windows = (2, 4, 8, 16)
norm_eps = 1e-06
clamp_limit = 7.0
sigmoid_slope = 1.702

BF = jnp.bfloat16
F32 = jnp.float32

NZ, NC, NY, NX = 16, 2, 4, 4
CAP = 32
LANE = 128
CHUNKS = 8
NEAR = 5
RIM = 16
WZ = 4
BACK = 1
ORDER = (
    ("w1",), ("w2",), ("ag1", 0), ("w3",), ("ag1", 1), ("ag2", 0, 0), ("ag2", 0, 1), ("ag1", 2), ("w4",),
    ("ag1", 3), ("ag3", 0), ("ag2", 1, 0), ("ag2", 1, 1), ("ag2", 2, 0), ("ag2", 2, 1), ("ag1", 4), ("w5",),
    ("ag2", 3, 0), ("ag2", 3, 1), ("ag3", 2), ("ag2", 4, 0), ("ag2", 4, 1), ("ag1", 5), ("ag1", 6),
    ("ag1", 7), ("pm",), ("ag3", 1), ("ag3", 4), ("ag4", 0, 0), ("ag4", 0, 1), ("ag3", 3), ("ag2", 6, 0),
    ("ag2", 6, 1), ("ag4", 2, 0), ("ag4", 2, 1), ("w6",), ("ag2", 5, 0), ("ag2", 5, 1), ("ag2", 7, 0),
    ("ag2", 7, 1), ("ag4", 1, 0), ("ag4", 1, 1), ("ag4", 4, 0), ("ag4", 4, 1), ("ag4", 3, 0), ("ag4", 3, 1),
    ("ag3", 6), ("w7",), ("c1", 0), ("c2", 0), ("c1", 1), ("ag3", 5), ("ag3", 7), ("c2", 1), ("c1", 2),
    ("c2", 2), ("c1", 3), ("c2", 3), ("rs2", 1, 0), ("rs2", 1, 1), ("c1", 4), ("ag4", 6, 0), ("ag4", 6, 1),
    ("c2", 4), ("po",), ("wh",), ("rs2", 0, 0), ("rs2", 0, 1), ("ag4", 5, 0), ("ag4", 5, 1), ("rs2", 2, 0),
    ("rs2", 2, 1), ("rs2", 4, 0), ("rs2", 4, 1), ("ag4", 7, 0), ("ag4", 7, 1), ("c1", 6), ("rs2", 3, 0),
    ("rs2", 3, 1), ("c2", 6), ("rs3", 0), ("rs3", 1), ("c1", 5), ("rs3", 2), ("c2", 5), ("c1", 7),
    ("c2", 7), ("rs3", 4), ("rs3", 3), ("rs4", 0, 0), ("rs4", 0, 1), ("rs2", 6, 0), ("rs2", 6, 1),
    ("rs4", 1, 0), ("rs4", 1, 1), ("rs2", 5, 0), ("rs2", 5, 1), ("rs4", 2, 0), ("rs4", 2, 1), ("rs4", 3, 0),
    ("rs4", 3, 1), ("rs2", 7, 0), ("rs2", 7, 1), ("rs4", 4, 0), ("rs4", 4, 1), ("rs5", 0), ("rs3", 6),
    ("rs5", 1), ("rs5", 3), ("rs3", 5), ("rs5", 2), ("rs4", 5, 0), ("rs4", 5, 1), ("rs3", 7), ("rs5", 4),
    ("rs4", 6, 0), ("rs4", 6, 1), ("rs5", 5), ("rs4", 7, 0), ("rs4", 7, 1), ("rs5", 6), ("rs5", 7),
)


def dot(a, b):
    return jnp.dot(a, b, preferred_element_type=F32)


def kernel(
    branch,
    pool_w_h,
    group_gain_h,
    out_w,
    out_gain_h,
    ffn_in,
    ffn_gain_h,
    routes_h,
    weight_h,
    gate_w,
    up_w,
    down_w,
    mixer_out,
    expert_out,
    pool_w,
    group_gain,
    out_gain,
    ffn_gain,
    routes_t,
    weight_t,
    full,
    full_w,
    gate_up,
    down,
    ext,
    mixed,
    proj,
    mixer,
    tokens,
    hot,
    picked,
    part,
    rx1,
    rx2,
    sum_x,
    ry1,
    ry2,
    home,
    result,
    answer,
    hidden,
    w_hi,
    w_lo,
    ag_s,
    ag_r,
    rs_s,
    rs_r,
    w_s,
    w_r,
    z_s,
    z_r,
    back_s,
    back_r,
    own_s,
    rim_s,
    load_s,
):
    z, c = lax.axis_index("z"), lax.axis_index("c")
    y, x = lax.axis_index("y"), lax.axis_index("x")
    ep = z * NC + c
    tp = y * NX + x
    tp_p = x * NY + y
    rows_a = branch.shape[0]
    rows_b = ffn_in.shape[0]
    model = ffn_in.shape[1]
    hid = gate_w.shape[2]
    width = branch.shape[1]
    slots = NZ * NC * CAP
    crow = slots // CHUNKS
    half = crow // 2
    per = NZ // CHUNKS
    wide = NY * LANE
    wrow = width // (NC * WZ)

    spot = (ep * NY + y) * NX + x
    total = NZ * NC * NY * NX

    def place(index):
        return (index // (NC * NY * NX), (index // (NY * NX)) % NC, (index // NX) % NY, index % NX)

    after = place((spot + 1) % total)
    before = place((spot + total - 1) % total)
    x_to = ((z, c, y, (x + 1) % NX), (z, c, y, (x + NX - 1) % NX))
    y_to = ((z, c, (y + 1) % NY, x), (z, c, (y + NY - 1) % NY, x))
    z_to = (((z + 1) % NZ, c, y, x), ((z + NZ - 1) % NZ, c, y, x))
    partner = (z, 1 - c, y, x)
    axis_x = (x, x_to)
    axis_y = (y, y_to)

    def order(g):
        return (axis_x, axis_y) if g % 2 == 0 else (axis_y, axis_x)

    def order_back(g):
        return (axis_x, axis_y) if g % 2 == BACK else (axis_y, axis_x)

    def index_of(seat):
        q = seat // per
        return (q if q < NEAR else CHUNKS - 1 + NEAR - q) * per + seat % per

    seat_of = index_of

    def step_z(i):
        return (z + NZ + ((i + 1) // 2) * (2 * (i % 2) - 1)) % NZ

    barrier = pltpu.get_barrier_semaphore()

    def greet(i, carry):
        zz = step_z(i)
        for cc in range(NC):
            pl.semaphore_signal(barrier, inc=1, device_id=(zz, cc, y, x), device_id_type=MESH)
        return carry

    for peer in (*x_to, *y_to, after, before, partner):
        pl.semaphore_signal(barrier, inc=1, device_id=peer, device_id_type=MESH)
    lax.fori_loop(1, NZ, greet, 0)

    loads = {}

    def load(name, src, dst):
        copy = pltpu.make_async_copy(src, dst, load_s.at[len(loads)])
        copy.start()
        loads[name] = copy

    own_cols = pl.ds(pl.multiple_of(tp * LANE, LANE), LANE)
    w_rows = pl.ds(pl.multiple_of((c * WZ + z % WZ) * wrow, wrow), wrow)
    load("tokens", ffn_in, tokens)
    load("ffn_gain", ffn_gain_h, ffn_gain)
    load("routes", routes_h, routes_t)
    load("weight", weight_h, weight_t)
    load("out_w", out_w.at[w_rows], full_w.at[w_rows, own_cols])
    load("branch", branch, ext.at[pl.ds(RIM, rows_a)])
    load("pool_w", pool_w_h, pool_w)
    load("group_gain", group_gain_h, group_gain)
    load("out_gain", out_gain_h, out_gain)

    for a in range(NY):
        for b in range(NX):
            here, there = (a * NX + b) * LANE, (b * NY + a) * LANE
            load(("down", 0, a, b), down_w.at[0, :, pl.ds(here, LANE)], down.at[1, :, pl.ds(there, LANE)])
            for k, w in enumerate((gate_w, up_w)):
                load(
                    ("gate_up", k, a, b),
                    w.at[0, pl.ds(here, LANE)],
                    gate_up.at[1, pl.ds(there, LANE), pl.ds(k * hid, hid)],
                )
    load(("down", 1), down_w.at[0], down.at[0])
    for k, w in enumerate((gate_w, up_w)):
        load(("gate_up", k), w.at[0], gate_up.at[0, :, pl.ds(k * hid, hid)])

    loads["tokens"].wait()
    acc = jnp.zeros((rows_b, LANE), F32)
    for k in range(model // LANE):
        v = tokens[:, k * LANE : (k + 1) * LANE].astype(F32)
        acc = acc + v * v
    scale = lax.rsqrt(jnp.sum(acc, axis=1, keepdims=True) * (1.0 / model) + norm_eps)
    loads["ffn_gain"].wait()
    normed = (tokens[:, own_cols].astype(F32) * scale * ffn_gain[:, own_cols]).astype(BF)

    loads["routes"].wait()
    loads["weight"].wait()
    experts = NZ * NC
    ids = lax.broadcasted_iota(jnp.int32, (experts, rows_b), 0)
    named = jnp.zeros((experts, rows_b), F32)
    weight = jnp.zeros((experts, rows_b), F32)
    for k in range(routes_t.shape[0]):
        hit = ids == routes_t[k : k + 1, :]
        named = named + jnp.where(hit, 1.0, 0.0)
        weight = weight + jnp.where(hit, weight_t[k : k + 1, :], 0.0)
    earlier = jnp.where(
        lax.broadcasted_iota(jnp.int32, (rows_b, rows_b), 0)
        < lax.broadcasted_iota(jnp.int32, (rows_b, rows_b), 1),
        1.0,
        0.0,
    ).astype(BF)
    place_of = jnp.where(named > 0.5, dot(named.astype(BF), earlier), -1.0)
    slot_ids = lax.broadcasted_iota(jnp.int32, (CAP, rows_b), 0).astype(F32)
    for e in range(experts):
        hot[e * CAP : (e + 1) * CAP, :] = jnp.where(slot_ids == place_of[e : e + 1, :], 1.0, 0.0).astype(BF)
    picked[...] = dot(hot[...], normed).astype(BF)
    loads["out_w"].wait()
    loads["branch"].wait()

    pl.semaphore_wait(barrier, 2 * (NZ - 1) + 7)

    sends = []

    def push(src, dst, sems, index, peer):
        send, recv = sems
        copy = pltpu.make_async_remote_copy(
            src,
            dst,
            send_sem=send.at[index],
            recv_sem=recv.at[index],
            device_id=peer,
            device_id_type=MESH,
        )
        copy.start()
        sends.append(copy)
        return copy

    def lanes(which, count):
        return pl.ds(pl.multiple_of(which * count, count), count)

    gather = {}

    def w_block(k, d=None, where=0):
        first, count = (c * WZ + (z + (k if where == 2 else 0) + NZ) % WZ) * wrow, wrow
        if d is not None:
            first, count = first + d * (wrow // 2), wrow // 2
        rows = pl.ds(pl.multiple_of(first, count), count)
        if where == 0:
            return full_w.at[rows, lanes(y * NX + (x + k + NX) % NX, LANE)]
        if where == 1:
            return full_w.at[rows, lanes((y + k + NY) % NY, wide)]
        return full_w.at[rows]

    w_axes = (x_to, y_to, z_to)

    def w_first(where):
        ref = w_block(0, None, where)
        gather["w", where, 0] = [
            push(ref, ref, (w_s, w_r), where * 4 + d, w_axes[where][d]) for d in range(2)
        ]

    def w_second(where):
        out = []
        for d in range(2):
            gather["w", where, 0][d].wait_recv()
            ref = w_block(2 * d - 1, d, where)
            out.append(push(ref, ref, (w_s, w_r), where * 4 + 2 + d, w_axes[where][d]))
        gather["w", where, 1] = out

    def w_third(where):
        for d in range(2):
            gather["w", where, 1][d].wait_recv()

    def w1():
        w_first(0)

    def w2():
        w_second(0)

    def w3():
        w_third(0)
        w_first(1)

    def w4():
        w_second(1)

    def w5():
        w_third(1)
        w_first(2)

    def w6():
        w_second(2)

    def w7():
        w_third(2)
        ref = full_w.at[lanes(c, width // NC)]
        gather["swap"] = push(ref, ref, (w_s, w_r), 12, partner)

    def ag1(g):
        arrived(g)
        (a, a_to), (b, b_to) = order(g)
        rows = pl.ds(g * crow, crow)
        ref = full.at[rows, lanes(b * NX + a, LANE)]
        gather[g, 0] = [push(ref, ref, (ag_s, ag_r), g * 8 + d, a_to[d]) for d in range(2)]

    def ag2(g, d):
        (a, a_to), (b, b_to) = order(g)
        gather[g, 0][d].wait_recv()
        rows = pl.ds(g * crow + d * half, half)
        ref = full.at[rows, lanes(b * NX + (a + NX - 1 + 2 * d) % NX, LANE)]
        gather[g, 1, d] = push(ref, ref, (ag_s, ag_r), g * 8 + 2 + d, a_to[d])

    def ag3(g):
        (a, a_to), (b, b_to) = order(g)
        for d in range(2):
            gather[g, 1, d].wait_recv()
        ref = full.at[pl.ds(g * crow, crow), lanes(b, wide)]
        gather[g, 2] = [push(ref, ref, (ag_s, ag_r), g * 8 + 4 + d, b_to[d]) for d in range(2)]

    def ag4(g, d):
        (a, a_to), (b, b_to) = order(g)
        gather[g, 2][d].wait_recv()
        rows = pl.ds(g * crow + d * half, half)
        ref = full.at[rows, lanes((b + NY - 1 + 2 * d) % NY, wide)]
        gather[g, 3, d] = push(ref, ref, (ag_s, ag_r), g * 8 + 6 + d, b_to[d])

    def seat_ref(seat, cc):
        cols = lanes(tp_p if (seat // per) % 2 else tp, LANE)
        return full.at[lanes(seat * NC + cc, CAP), cols]

    own_pick = pltpu.make_async_copy(picked.at[lanes(ep, CAP)], seat_ref(seat_of(0), c), own_s.at[0])

    def dispatch(zz, cc, seat):
        return pltpu.make_async_remote_copy(
            picked.at[lanes(zz * NC + cc, CAP)],
            seat_ref(seat, c),
            send_sem=z_s.at[0],
            recv_sem=z_r.at[seat // per],
            device_id=(zz, cc, y, x),
            device_id_type=MESH,
        )

    def dispatch_all():
        for seat in range(NZ):
            i = index_of(seat)
            if i == 0:
                own_pick.start()
                dispatch(z, 1 - c, seat).start()
                continue
            back = min(i + 2 * (i % 2) - 1, NZ - 1)
            for cc in range(NC):
                dispatch(step_z(i), cc, seat_of(back)).start()

    def arrived(g):
        own = g == seat_of(0) // per
        ref = full.at[pl.ds(g * crow, crow - CAP if own else crow), 0:LANE]
        pltpu.make_async_copy(ref, ref, z_r.at[g]).wait()
        if own:
            own_pick.wait()

    def pool_mix():
        gather["rim"].wait_recv()
        for name in ("pool_w", "group_gain", "out_gain"):
            loads[name].wait()
        reach = rows_a + RIM
        row = lax.broadcasted_iota(jnp.int32, (rows_a, reach), 0) + RIM
        col = lax.broadcasted_iota(jnp.int32, (rows_a, reach), 1)
        first = jnp.where(spot == 0, RIM, 0)
        age = jnp.where(col < first, reach, row - col)
        position = spot * rows_a + lax.broadcasted_iota(jnp.int32, (rows_a, LANE), 0)
        parts = []
        acc = jnp.zeros((rows_a, LANE), F32)
        for k, window in enumerate(pool_windows):
            cols = slice(k * LANE, (k + 1) * LANE)
            band = jnp.where((age >= 0) & (age < window), 1.0, 0.0).astype(BF)
            summed = dot(band, ext[:, cols])
            count = jnp.minimum(position + 1, window).astype(F32)
            pooled = (summed / count - ext[RIM:, cols].astype(F32)).astype(BF)
            mix = dot(pooled, pool_w[k])
            parts.append(mix)
            acc = acc + mix * mix
        scale = lax.rsqrt(jnp.sum(acc, axis=1, keepdims=True) * (1.0 / width) + norm_eps)
        for k, mix in enumerate(parts):
            cols = slice(k * LANE, (k + 1) * LANE)
            mixed[:, cols] = (mix * scale * group_gain[:, cols]).astype(BF)

    store = pltpu.make_async_copy(mixer, mixer_out, own_s.at[2])

    def pool_out():
        gather["swap"].wait_recv()
        acc = jnp.zeros((rows_a, LANE), F32)
        tile = 256
        for n in range(model // tile):
            cols = slice(n * tile, (n + 1) * tile)
            v = dot(mixed[...], full_w[:, cols])
            proj[:, cols] = v
            for k in range(tile // LANE):
                w = v[:, k * LANE : (k + 1) * LANE]
                acc = acc + w * w
        scale = lax.rsqrt(jnp.sum(acc, axis=1, keepdims=True) * (1.0 / model) + norm_eps)
        for n in range(model // tile):
            cols = slice(n * tile, (n + 1) * tile)
            mixer[:, cols] = (proj[:, cols] * scale * out_gain[:, cols]).astype(BF)
        store.start()

    def weigh():
        for e in range(0, experts, LANE // CAP):
            rows = []
            for k in range(LANE // CAP):
                h = hot[(e + k) * CAP : (e + k + 1) * CAP, :].astype(F32)
                rows.append(h * weight[e + k : e + k + 1, :])
            turned = jnp.concatenate(rows, axis=0).T
            high = turned.astype(BF)
            cols = slice(e * CAP, e * CAP + LANE)
            w_hi[:, cols] = high
            w_lo[:, cols] = (turned - high.astype(F32)).astype(BF)

    reduce = {}

    def block(which, count):
        return lanes(which % NX, count)

    def down_block(g, k):
        (a, a_to), (b, b_to) = order_back(g)
        rows, cols = pl.ds(g * crow, crow), block(a + 2 + k, wide)
        part[rows, cols] = dot(hidden[rows, :], down[1 if g % 2 == BACK else 0, :, cols]).astype(BF)
        return cols

    def c1(g):
        (a, a_to), (b, b_to) = order_back(g)
        for d in range(2):
            gather[g, 3, d].wait_recv()
        for name in tuple(loads):
            if isinstance(name, tuple):
                loads.pop(name).wait()
        r = g * crow
        both = dot(full[r : r + crow, :], gate_up[g % 2])
        gate = jnp.minimum(both[:, :hid], clamp_limit)
        up = jnp.clip(both[:, hid:], -clamp_limit, clamp_limit)
        hidden[r : r + crow, :] = ((up + 1.0) * gate * jax.nn.sigmoid(sigmoid_slope * gate)).astype(BF)
        cols = down_block(g, 0)
        reduce[g, 0] = [
            push(
                part.at[pl.ds(r + d * half, half), cols],
                rx1.at[pl.ds(r + d * half, half)],
                (rs_s, rs_r),
                g * 8 + d,
                a_to[d],
            )
            for d in range(2)
        ]

    def c2(g):
        for k in range(1, NX):
            down_block(g, k)

    def add(*values):
        out = values[0].astype(F32)
        for v in values[1:]:
            out = out + v.astype(F32)
        return out.astype(BF)

    def rs2(g, d):
        (a, a_to), (b, b_to) = order_back(g)
        r = g * crow
        reduce[g, 0][d].wait_recv()
        cols = block(a + 1 + 2 * d, wide)
        rows = slice(r + d * half, r + d * half + half)
        part[rows, cols] = add(part[rows, cols], rx1[rows, :])
        reduce[g, 1, d] = push(
            part.at[pl.ds(r, crow), cols],
            rx2.at[pl.ds(r, crow), pl.ds(d * wide, wide)],
            (rs_s, rs_r),
            g * 8 + 2 + d,
            a_to[d],
        )

    def rs3(g):
        (a, a_to), (b, b_to) = order_back(g)
        r = g * crow
        for d in range(2):
            reduce[g, 1, d].wait_recv()
        rows = slice(r, r + crow)
        sum_x[rows, :] = add(part[rows, block(a, wide)], rx2[rows, :wide], rx2[rows, wide:])
        cols = block(b + 2, LANE)
        reduce[g, 2] = [
            push(
                sum_x.at[pl.ds(r + d * half, half), cols],
                ry1.at[pl.ds(r + d * half, half)],
                (rs_s, rs_r),
                g * 8 + 4 + d,
                b_to[d],
            )
            for d in range(2)
        ]

    def rs4(g, d):
        (a, a_to), (b, b_to) = order_back(g)
        r = g * crow
        reduce[g, 2][d].wait_recv()
        cols = block(b + 1 + 2 * d, LANE)
        rows = slice(r + d * half, r + d * half + half)
        sum_x[rows, cols] = add(sum_x[rows, cols], ry1[rows, :])
        reduce[g, 3, d] = push(
            sum_x.at[pl.ds(r, crow), cols],
            ry2.at[pl.ds(r, crow), pl.ds(d * LANE, LANE)],
            (rs_s, rs_r),
            g * 8 + 6 + d,
            b_to[d],
        )

    own_rows = lanes(ep, CAP)
    own_back = pltpu.make_async_copy(
        home.at[lanes(seat_of(0) * NC + c, CAP)], result.at[own_rows], own_s.at[1]
    )

    def give_back(seat, cc):
        return pltpu.make_async_remote_copy(
            home.at[lanes(seat * NC + cc, CAP)],
            result.at[own_rows],
            send_sem=back_s.at[0],
            recv_sem=back_r.at[0],
            device_id=(step_z(index_of(seat)), cc, y, x),
            device_id_type=MESH,
        )

    def rs5(g):
        (a, a_to), (b, b_to) = order_back(g)
        r = g * crow
        for d in range(2):
            reduce[g, 3, d].wait_recv()
        rows = slice(r, r + crow)
        home[rows, :] = add(sum_x[rows, block(b, LANE)], ry2[rows, :LANE], ry2[rows, LANE:])
        for seat in range(g * per, (g + 1) * per):
            if index_of(seat) == 0:
                own_back.start()
                give_back(seat, 1 - c).start()
                continue
            for cc in range(NC):
                give_back(seat, cc).start()

    gather["rim"] = push(ext.at[pl.ds(rows_a, RIM)], ext.at[pl.ds(0, RIM)], (w_s, w_r), 13, after)
    dispatch_all()

    steps = dict(
        w1=w1, w2=w2, w3=w3, w4=w4, w5=w5, w6=w6, w7=w7, pm=pool_mix, po=pool_out,
        ag1=ag1, ag2=ag2, ag3=ag3, ag4=ag4, c1=c1, c2=c2, rs2=rs2, rs3=rs3, rs4=rs4, rs5=rs5, wh=weigh,
    )
    for name, *where in ORDER:
        steps[name](*where)

    store.wait()
    own_back.wait()
    ref = result.at[pl.ds(0, slots - CAP)]
    pltpu.make_async_copy(ref, ref, back_r.at[0]).wait()
    value = dot(w_hi[...], result[...]) + dot(w_lo[...], result[...])
    answer[...] = value.astype(BF)
    last = pltpu.make_async_copy(answer, expert_out, own_s.at[3])
    last.start()
    for copy in sends:
        copy.wait_send()
    ref = picked.at[pl.ds(0, slots - CAP)]
    pltpu.make_async_copy(ref, ref, z_s.at[0]).wait()
    ref = home.at[pl.ds(0, slots - CAP)]
    pltpu.make_async_copy(ref, ref, back_s.at[0]).wait()
    last.wait()


def per_device(
    branch_in,
    pool_weight,
    group_gain,
    out_weight,
    out_gain,
    ffn_input,
    ffn_gain,
    routes,
    route_weight,
    gate_weight,
    up_weight,
    down_weight,
):
    rows_a, width = branch_in.shape
    rows_b, model = ffn_input.shape
    hid = gate_weight.shape[2]
    top = routes.shape[1]
    slots = NZ * NC * CAP
    wide = NY * LANE
    any_ = pl.BlockSpec(memory_space=pl.ANY)
    dma = pltpu.SemaphoreType.DMA
    return pl.pallas_call(
        kernel,
        name="mixer_and_experts",
        out_shape=(
            jax.ShapeDtypeStruct((rows_a, model), BF),
            jax.ShapeDtypeStruct((rows_b, LANE), BF),
        ),
        in_specs=[any_] * 12,
        out_specs=(any_, any_),
        scratch_shapes=[
            pltpu.VMEM(pool_weight.shape, BF),
            pltpu.VMEM((1, width), F32),
            pltpu.VMEM((1, model), F32),
            pltpu.VMEM((1, model), F32),
            pltpu.VMEM((top, rows_b), jnp.int32),
            pltpu.VMEM((top, rows_b), F32),
            pltpu.VMEM((slots, model), BF),
            pltpu.VMEM((width, model), BF),
            pltpu.VMEM((2, model, 2 * hid), BF),
            pltpu.VMEM((2, hid, model), BF),
            pltpu.VMEM((rows_a + RIM, width), BF),
            pltpu.VMEM((rows_a, width), BF),
            pltpu.VMEM((rows_a, model), F32),
            pltpu.VMEM((rows_a, model), BF),
            pltpu.VMEM((rows_b, model), BF),
            pltpu.VMEM((slots, rows_b), BF),
            pltpu.VMEM((slots, LANE), BF),
            pltpu.VMEM((slots, model), BF),
            pltpu.VMEM((slots, wide), BF),
            pltpu.VMEM((slots, 2 * wide), BF),
            pltpu.VMEM((slots, wide), BF),
            pltpu.VMEM((slots, LANE), BF),
            pltpu.VMEM((slots, 2 * LANE), BF),
            pltpu.VMEM((slots, LANE), BF),
            pltpu.VMEM((slots, LANE), BF),
            pltpu.VMEM((rows_b, LANE), BF),
            pltpu.VMEM((slots, hid), BF),
            pltpu.VMEM((rows_b, slots), BF),
            pltpu.VMEM((rows_b, slots), BF),
            dma((CHUNKS * 8,)),
            dma((CHUNKS * 8,)),
            dma((CHUNKS * 8,)),
            dma((CHUNKS * 8,)),
            dma((14,)),
            dma((14,)),
            dma((1,)),
            dma((CHUNKS,)),
            dma((1,)),
            dma((1,)),
            dma((4,)),
            dma((2,)),
            dma((64,)),
        ],
        compiler_params=pltpu.CompilerParams(collective_id=0, has_side_effects=True),
    )(
        branch_in,
        pool_weight,
        group_gain[None],
        out_weight,
        out_gain[None],
        ffn_input,
        ffn_gain[None],
        routes.T,
        route_weight.T,
        gate_weight,
        up_weight,
        down_weight,
    )


def solution(mesh):
    split = Mesh(mesh.devices.reshape(NZ, NC, NY, NX), AXES)
    in_specs = (
        P(AXES, None),
        P(),
        P(),
        P(None, TP),
        P(),
        P(EP, None),
        P(),
        P(EP, None),
        P(EP, None),
        P(EP, None, TP),
        P(EP, None, TP),
        P(EP, TP, None),
    )
    out_specs = (P(AXES, None), P(EP, TP))
    return jax.shard_map(
        per_device, mesh=split, in_specs=in_specs, out_specs=out_specs, check_vma=False
    )
```

time: 109 us -> 100 us (0.917)
  Pallas kernels: 105 us -> 96.3 us
    pallas_call x1, Pallas kernels: 105 us -> 96.3 us  [per_device(): pl.pallas_call(kernel, name='mixer_and_experts', out_shape=(jax.ShapeDtyp...]
where the time goes in v2:
time: 100 us; the launch traced here: 99.9 us
  Pallas kernels  96.3 us (96%)
  local copies, waits for them, and re-layouts  2.93 us (3%)
    pallas_call x1, Pallas kernels, per_device(): pl.pallas_call(kernel, name='mixer_and_experts', out_shape=(jax.ShapeDtyp...  96.3 us
    unnamed x4, local copies, waits for them, and re-layouts  2.93 us

profile of v2, /device:TPU:1, one launch (start us, length us, event | category | flops | bytes accessed | tf_op | source)
XLA Modules:
  0.0 99.9 jit_solution(2030415486423223934)
XLA Ops:
  0.6 96.3 %mixer_and_experts.1 = (bf16[256,2048]{1,0:T(8,128)(2,1)}, bf16[128,128]{1,0:T(8,128)(2,1)}) custom-call(bf16[256,512]{1,0:T(8,128)(2,1)} %branch.1, bf16[4,128,128]{2,1,0:T(8,128)(2,1)} %pool_w_h.1, f32[1,512]{1,0:T(1,128)} %bitcast.7, bf16[512,128]{1,0:T(8,128)(2,1)} %out_w.1, f32[1,2048]{1,0:T(1,128)} %bitcast.5, bf16[128,2048]{1,0:T(8,128)(2,1)} %ffn_in.1, ...), custom_call_target="tpu_custom_call" | custom-call | tf_op jit(solution)/shard_map/mixer_and_experts/pallas_call | solution.py:610
  96.9 0.0 copy-start
  96.9 2.3 %copy.16 = bf16[256,2048]{1,0:T(8,128)(2,1)} copy(bf16[256,2048]{1,0:T(8,128)(2,1)} %get-tuple-element.4) | data formatting | bytes 2097152
  99.3 0.0 copy-done
  99.3 0.6 copy.17
Async XLA Ops:
  96.9 2.3 %copy-start = (bf16[128,128]{1,0:T(8,128)(2,1)S(1)}, bf16[128,128]{1,0:T(8,128)(2,1)}, u32[]{:S(2)}) copy-start(bf16[128,128]{1,0:T(8,128)(2,1)} %get-tuple-element.5) | copy-start | bytes 98308

commit v3 on v2

--- a/solution.py
+++ b/solution.py
@@ -25,27 +25,29 @@
 CAP = 32
 LANE = 128
 CHUNKS = 8
-NEAR = 5
+NEAR = 8
+SHARED = {"down": 9, "gate_up": 10}
 RIM = 16
 WZ = 4
 BACK = 1
 ORDER = (
-    ("w1",), ("w2",), ("ag1", 0), ("w3",), ("ag1", 1), ("ag2", 0, 0), ("ag2", 0, 1), ("ag1", 2), ("w4",),
-    ("ag1", 3), ("ag3", 0), ("ag2", 1, 0), ("ag2", 1, 1), ("ag2", 2, 0), ("ag2", 2, 1), ("ag1", 4), ("w5",),
-    ("ag2", 3, 0), ("ag2", 3, 1), ("ag3", 2), ("ag2", 4, 0), ("ag2", 4, 1), ("ag1", 5), ("ag1", 6),
-    ("ag1", 7), ("pm",), ("ag3", 1), ("ag3", 4), ("ag4", 0, 0), ("ag4", 0, 1), ("ag3", 3), ("ag2", 6, 0),
-    ("ag2", 6, 1), ("ag4", 2, 0), ("ag4", 2, 1), ("w6",), ("ag2", 5, 0), ("ag2", 5, 1), ("ag2", 7, 0),
-    ("ag2", 7, 1), ("ag4", 1, 0), ("ag4", 1, 1), ("ag4", 4, 0), ("ag4", 4, 1), ("ag4", 3, 0), ("ag4", 3, 1),
-    ("ag3", 6), ("w7",), ("c1", 0), ("c2", 0), ("c1", 1), ("ag3", 5), ("ag3", 7), ("c2", 1), ("c1", 2),
-    ("c2", 2), ("c1", 3), ("c2", 3), ("rs2", 1, 0), ("rs2", 1, 1), ("c1", 4), ("ag4", 6, 0), ("ag4", 6, 1),
-    ("c2", 4), ("po",), ("wh",), ("rs2", 0, 0), ("rs2", 0, 1), ("ag4", 5, 0), ("ag4", 5, 1), ("rs2", 2, 0),
-    ("rs2", 2, 1), ("rs2", 4, 0), ("rs2", 4, 1), ("ag4", 7, 0), ("ag4", 7, 1), ("c1", 6), ("rs2", 3, 0),
-    ("rs2", 3, 1), ("c2", 6), ("rs3", 0), ("rs3", 1), ("c1", 5), ("rs3", 2), ("c2", 5), ("c1", 7),
-    ("c2", 7), ("rs3", 4), ("rs3", 3), ("rs4", 0, 0), ("rs4", 0, 1), ("rs2", 6, 0), ("rs2", 6, 1),
-    ("rs4", 1, 0), ("rs4", 1, 1), ("rs2", 5, 0), ("rs2", 5, 1), ("rs4", 2, 0), ("rs4", 2, 1), ("rs4", 3, 0),
-    ("rs4", 3, 1), ("rs2", 7, 0), ("rs2", 7, 1), ("rs4", 4, 0), ("rs4", 4, 1), ("rs5", 0), ("rs3", 6),
-    ("rs5", 1), ("rs5", 3), ("rs3", 5), ("rs5", 2), ("rs4", 5, 0), ("rs4", 5, 1), ("rs3", 7), ("rs5", 4),
-    ("rs4", 6, 0), ("rs4", 6, 1), ("rs5", 5), ("rs4", 7, 0), ("rs4", 7, 1), ("rs5", 6), ("rs5", 7),
+    ("ag1", 0), ("ag1", 1), ("ag2", 0, 0), ("ag2", 0, 1), ("ag1", 2), ("ag2", 1, 0), ("ag2", 1, 1), ("w2",),
+    ("ag3", 0), ("ag1", 3), ("ag1", 4), ("ag2", 2, 0), ("ag2", 2, 1), ("ag3", 1), ("ag1", 5), ("ag4", 0, 0),
+    ("ag4", 0, 1), ("ag1", 6), ("ag1", 7), ("ag2", 3, 0), ("ag2", 3, 1), ("ag3", 2), ("ag4", 1, 0),
+    ("ag4", 1, 1), ("pm",), ("ag2", 5, 0), ("ag2", 5, 1), ("w3",), ("ag2", 6, 0), ("ag2", 6, 1),
+    ("ag2", 4, 0), ("ag3", 3), ("ag2", 7, 0), ("ag2", 7, 1), ("ag2", 4, 1), ("ag3", 5), ("ag4", 2, 0),
+    ("ag4", 2, 1), ("ag3", 6), ("ag4", 3, 1), ("ag4", 3, 0), ("ag3", 7), ("ag3", 4), ("c1", 1),
+    ("ag4", 5, 0), ("c1", 0), ("ag4", 5, 1), ("c2", 0), ("w4",), ("c2", 1), ("ag4", 6, 0), ("ag4", 6, 1),
+    ("ag4", 7, 0), ("ag4", 7, 1), ("ag4", 4, 0), ("ag4", 4, 1), ("c1", 3), ("c2", 3), ("rs2", 0, 0),
+    ("rs2", 0, 1), ("c1", 5), ("c2", 5), ("c1", 7), ("c2", 7), ("c1", 6), ("rs2", 3, 0), ("rs2", 3, 1),
+    ("c2", 6), ("w5",), ("c1", 4), ("c2", 4), ("rs3", 0), ("c1", 2), ("c2", 2), ("rs2", 7, 0),
+    ("rs2", 7, 1), ("rs2", 6, 0), ("rs2", 6, 1), ("rs3", 3), ("rs4", 0, 0), ("rs4", 0, 1), ("rs2", 5, 0),
+    ("rs2", 5, 1), ("rs2", 4, 0), ("rs2", 4, 1), ("rs3", 7), ("rs5", 0), ("rs3", 6), ("rs4", 3, 0),
+    ("rs4", 3, 1), ("rs2", 1, 0), ("rs2", 1, 1), ("rs2", 2, 0), ("rs2", 2, 1), ("rs3", 5), ("w6",),
+    ("rs4", 6, 0), ("rs4", 6, 1), ("rs3", 4), ("rs4", 7, 0), ("rs4", 7, 1), ("rs5", 3), ("rs3", 1),
+    ("rs5", 6), ("rs4", 4, 0), ("rs4", 4, 1), ("rs3", 2), ("rs4", 5, 0), ("rs4", 5, 1), ("rs5", 7),
+    ("rs4", 1, 0), ("rs4", 1, 1), ("rs5", 4), ("rs4", 2, 0), ("rs4", 2, 1), ("rs5", 5), ("rs5", 1), ("w7",),
+    ("rs5", 2), ("po",), ("wh",),
 )
 
 
@@ -108,7 +110,6 @@
     back_s,
     back_r,
     own_s,
-    rim_s,
     load_s,
 ):
     z, c = lax.axis_index("z"), lax.axis_index("c")
@@ -173,9 +174,10 @@
     loads = {}
 
     def load(name, src, dst):
-        copy = pltpu.make_async_copy(src, dst, load_s.at[len(loads)])
+        copy = pltpu.make_async_copy(src, dst, load_s.at[SHARED.get(name, len(loads))])
         copy.start()
-        loads[name] = copy
+        if name not in SHARED:
+            loads[name] = copy
 
     own_cols = pl.ds(pl.multiple_of(tp * LANE, LANE), LANE)
     w_rows = pl.ds(pl.multiple_of((c * WZ + z % WZ) * wrow, wrow), wrow)
@@ -192,16 +194,16 @@
     for a in range(NY):
         for b in range(NX):
             here, there = (a * NX + b) * LANE, (b * NY + a) * LANE
-            load(("down", 0, a, b), down_w.at[0, :, pl.ds(here, LANE)], down.at[1, :, pl.ds(there, LANE)])
+            load("down", down_w.at[0, :, pl.ds(here, LANE)], down.at[1, :, pl.ds(there, LANE)])
             for k, w in enumerate((gate_w, up_w)):
                 load(
-                    ("gate_up", k, a, b),
+                    "gate_up",
                     w.at[0, pl.ds(here, LANE)],
                     gate_up.at[1, pl.ds(there, LANE), pl.ds(k * hid, hid)],
                 )
-    load(("down", 1), down_w.at[0], down.at[0])
+    load("down", down_w.at[0], down.at[0])
     for k, w in enumerate((gate_w, up_w)):
-        load(("gate_up", k), w.at[0], gate_up.at[0, :, pl.ds(k * hid, hid)])
+        load("gate_up", w.at[0], gate_up.at[0, :, pl.ds(k * hid, hid)])
 
     loads["tokens"].wait()
     acc = jnp.zeros((rows_b, LANE), F32)
@@ -238,20 +240,17 @@
 
     pl.semaphore_wait(barrier, 2 * (NZ - 1) + 7)
 
-    sends = []
-
     def push(src, dst, sems, index, peer):
-        send, recv = sems
+        (send, recv), (out, into) = sems, index
         copy = pltpu.make_async_remote_copy(
             src,
             dst,
-            send_sem=send.at[index],
-            recv_sem=recv.at[index],
+            send_sem=send.at[out],
+            recv_sem=recv.at[into],
             device_id=peer,
             device_id_type=MESH,
         )
         copy.start()
-        sends.append(copy)
         return copy
 
     def lanes(which, count):
@@ -275,7 +274,7 @@
     def w_first(where):
         ref = w_block(0, None, where)
         gather["w", where, 0] = [
-            push(ref, ref, (w_s, w_r), where * 4 + d, w_axes[where][d]) for d in range(2)
+            push(ref, ref, (w_s, w_r), (where, where * 4 + d), w_axes[where][d]) for d in range(2)
         ]
 
     def w_second(where):
@@ -283,7 +282,7 @@
         for d in range(2):
             gather["w", where, 0][d].wait_recv()
             ref = w_block(2 * d - 1, d, where)
-            out.append(push(ref, ref, (w_s, w_r), where * 4 + 2 + d, w_axes[where][d]))
+            out.append(push(ref, ref, (w_s, w_r), (where, where * 4 + 2 + d), w_axes[where][d]))
         gather["w", where, 1] = out
 
     def w_third(where):
@@ -313,35 +312,44 @@
     def w7():
         w_third(2)
         ref = full_w.at[lanes(c, width // NC)]
-        gather["swap"] = push(ref, ref, (w_s, w_r), 12, partner)
+        gather["swap"] = push(ref, ref, (w_s, w_r), (3, 12), partner)
+
+    def spread(g, which):
+        (a, a_to), (b, b_to) = order(g)
+        ref = full.at[pl.ds(g * crow, crow), lanes(b * NX + which % NX, LANE)]
+        for d in range(2):
+            push(ref, ref, (ag_s, ag_r), (0, g * 8 + 4 + d), b_to[d])
 
     def ag1(g):
         arrived(g)
         (a, a_to), (b, b_to) = order(g)
         rows = pl.ds(g * crow, crow)
         ref = full.at[rows, lanes(b * NX + a, LANE)]
-        gather[g, 0] = [push(ref, ref, (ag_s, ag_r), g * 8 + d, a_to[d]) for d in range(2)]
+        gather[g, 0] = [push(ref, ref, (ag_s, ag_r), (0, g * 8 + d), a_to[d]) for d in range(2)]
+        spread(g, a)
 
     def ag2(g, d):
         (a, a_to), (b, b_to) = order(g)
         gather[g, 0][d].wait_recv()
+        which = a + NX - 1 + 2 * d
         rows = pl.ds(g * crow + d * half, half)
-        ref = full.at[rows, lanes(b * NX + (a + NX - 1 + 2 * d) % NX, LANE)]
-        gather[g, 1, d] = push(ref, ref, (ag_s, ag_r), g * 8 + 2 + d, a_to[d])
+        ref = full.at[rows, lanes(b * NX + which % NX, LANE)]
+        gather[g, 1, d] = push(ref, ref, (ag_s, ag_r), (0, g * 8 + 2 + d), a_to[d])
+        spread(g, which)
 
     def ag3(g):
         (a, a_to), (b, b_to) = order(g)
         for d in range(2):
             gather[g, 1, d].wait_recv()
-        ref = full.at[pl.ds(g * crow, crow), lanes(b, wide)]
-        gather[g, 2] = [push(ref, ref, (ag_s, ag_r), g * 8 + 4 + d, b_to[d]) for d in range(2)]
+        spread(g, a + 2)
 
     def ag4(g, d):
         (a, a_to), (b, b_to) = order(g)
-        gather[g, 2][d].wait_recv()
+        row = full.at[pl.ds(g * crow, crow), 0:wide]
+        pltpu.make_async_copy(row, row, ag_r.at[g * 8 + 4 + d]).wait()
         rows = pl.ds(g * crow + d * half, half)
         ref = full.at[rows, lanes((b + NY - 1 + 2 * d) % NY, wide)]
-        gather[g, 3, d] = push(ref, ref, (ag_s, ag_r), g * 8 + 6 + d, b_to[d])
+        gather[g, 3, d] = push(ref, ref, (ag_s, ag_r), (0, g * 8 + 6 + d), b_to[d])
 
     def seat_ref(seat, cc):
         cols = lanes(tp_p if (seat // per) % 2 else tp, LANE)
@@ -449,9 +457,10 @@
         (a, a_to), (b, b_to) = order_back(g)
         for d in range(2):
             gather[g, 3, d].wait_recv()
-        for name in tuple(loads):
-            if isinstance(name, tuple):
-                loads.pop(name).wait()
+        if "weights" not in gather:
+            gather["weights"] = True
+            for ref, name in ((down, "down"), (gate_up, "gate_up")):
+                pltpu.make_async_copy(ref, ref, load_s.at[SHARED[name]]).wait()
         r = g * crow
         both = dot(full[r : r + crow, :], gate_up[g % 2])
         gate = jnp.minimum(both[:, :hid], clamp_limit)
@@ -463,7 +472,7 @@
                 part.at[pl.ds(r + d * half, half), cols],
                 rx1.at[pl.ds(r + d * half, half)],
                 (rs_s, rs_r),
-                g * 8 + d,
+                (0, g * 8 + d),
                 a_to[d],
             )
             for d in range(2)
@@ -490,7 +499,7 @@
             part.at[pl.ds(r, crow), cols],
             rx2.at[pl.ds(r, crow), pl.ds(d * wide, wide)],
             (rs_s, rs_r),
-            g * 8 + 2 + d,
+            (0, g * 8 + 2 + d),
             a_to[d],
         )
 
@@ -507,7 +516,7 @@
                 sum_x.at[pl.ds(r + d * half, half), cols],
                 ry1.at[pl.ds(r + d * half, half)],
                 (rs_s, rs_r),
-                g * 8 + 4 + d,
+                (0, g * 8 + 4 + d),
                 b_to[d],
             )
             for d in range(2)
@@ -524,7 +533,7 @@
             sum_x.at[pl.ds(r, crow), cols],
             ry2.at[pl.ds(r, crow), pl.ds(d * LANE, LANE)],
             (rs_s, rs_r),
-            g * 8 + 6 + d,
+            (0, g * 8 + 6 + d),
             b_to[d],
         )
 
@@ -558,11 +567,12 @@
             for cc in range(NC):
                 give_back(seat, cc).start()
 
-    gather["rim"] = push(ext.at[pl.ds(rows_a, RIM)], ext.at[pl.ds(0, RIM)], (w_s, w_r), 13, after)
+    gather["rim"] = push(ext.at[pl.ds(rows_a, RIM)], ext.at[pl.ds(0, RIM)], (w_s, w_r), (4, 13), after)
+    w1()
     dispatch_all()
 
     steps = dict(
-        w1=w1, w2=w2, w3=w3, w4=w4, w5=w5, w6=w6, w7=w7, pm=pool_mix, po=pool_out,
+        w2=w2, w3=w3, w4=w4, w5=w5, w6=w6, w7=w7, pm=pool_mix, po=pool_out,
         ag1=ag1, ag2=ag2, ag3=ag3, ag4=ag4, c1=c1, c2=c2, rs2=rs2, rs3=rs3, rs4=rs4, rs5=rs5, wh=weigh,
     )
     for name, *where in ORDER:
@@ -576,8 +586,16 @@
     answer[...] = value.astype(BF)
     last = pltpu.make_async_copy(answer, expert_out, own_s.at[3])
     last.start()
-    for copy in sends:
-        copy.wait_send()
+    for ref, sem in (
+        (full.at[:, 0 : 3 * LANE + 3 * wide], ag_s.at[0]),
+        (part.at[:, 0 : 3 * LANE + 3 * wide], rs_s.at[0]),
+        (full_w.at[pl.ds(0, 3 * wrow), 0:LANE], w_s.at[0]),
+        (full_w.at[pl.ds(0, 3 * wrow), 0:wide], w_s.at[1]),
+        (full_w.at[pl.ds(0, 3 * wrow)], w_s.at[2]),
+        (full_w.at[pl.ds(0, width // NC)], w_s.at[3]),
+        (ext.at[pl.ds(0, RIM)], w_s.at[4]),
+    ):
+        pltpu.make_async_copy(ref, ref, sem).wait()
     ref = picked.at[pl.ds(0, slots - CAP)]
     pltpu.make_async_copy(ref, ref, z_s.at[0]).wait()
     ref = home.at[pl.ds(0, slots - CAP)]
@@ -646,19 +664,18 @@
             pltpu.VMEM((slots, hid), BF),
             pltpu.VMEM((rows_b, slots), BF),
             pltpu.VMEM((rows_b, slots), BF),
+            dma((1,)),
             dma((CHUNKS * 8,)),
+            dma((1,)),
             dma((CHUNKS * 8,)),
-            dma((CHUNKS * 8,)),
-            dma((CHUNKS * 8,)),
-            dma((14,)),
+            dma((5,)),
             dma((14,)),
             dma((1,)),
             dma((CHUNKS,)),
             dma((1,)),
             dma((1,)),
             dma((4,)),
-            dma((2,)),
-            dma((64,)),
+            dma((11,)),
         ],
         compiler_params=pltpu.CompilerParams(collective_id=0, has_side_effects=True),
     )(

time: 100 us -> 89.7 us (0.90)
  Pallas kernels: 96.3 us -> 85.9 us
    pallas_call x1, Pallas kernels: 96.3 us -> 85.9 us  [per_device(): pl.pallas_call(kernel, name='mixer_and_experts', out_shape=(jax.ShapeDtyp...]
where the time goes in v3:
time: 89.7 us; the launch traced here: 89.5 us
  Pallas kernels  85.9 us (96%)
  local copies, waits for them, and re-layouts  2.93 us (3%)
    pallas_call x1, Pallas kernels, per_device(): pl.pallas_call(kernel, name='mixer_and_experts', out_shape=(jax.ShapeDtyp...  85.9 us
    unnamed x4, local copies, waits for them, and re-layouts  2.93 us

profile of v3, /device:TPU:1, one launch (start us, length us, event | category | flops | bytes accessed | tf_op | source)
XLA Modules:
  0.0 89.5 jit_solution(11962450094518874358)
XLA Ops:
  0.6 85.9 %mixer_and_experts.1 = (bf16[256,2048]{1,0:T(8,128)(2,1)}, bf16[128,128]{1,0:T(8,128)(2,1)}) custom-call(bf16[256,512]{1,0:T(8,128)(2,1)} %branch.1, bf16[4,128,128]{2,1,0:T(8,128)(2,1)} %pool_w_h.1, f32[1,512]{1,0:T(1,128)} %bitcast.7, bf16[512,128]{1,0:T(8,128)(2,1)} %out_w.1, f32[1,2048]{1,0:T(1,128)} %bitcast.5, bf16[128,2048]{1,0:T(8,128)(2,1)} %ffn_in.1, ...), custom_call_target="tpu_custom_call" | custom-call | tf_op jit(solution)/shard_map/mixer_and_experts/pallas_call | solution.py:628
  86.6 0.0 copy-start
  86.6 2.3 %copy.16 = bf16[256,2048]{1,0:T(8,128)(2,1)} copy(bf16[256,2048]{1,0:T(8,128)(2,1)} %get-tuple-element.4) | data formatting | bytes 2097152
  88.9 0.0 copy-done
  88.9 0.6 copy.17
Async XLA Ops:
  86.6 2.3 %copy-start = (bf16[128,128]{1,0:T(8,128)(2,1)S(1)}, bf16[128,128]{1,0:T(8,128)(2,1)}, u32[]{:S(2)}) copy-start(bf16[128,128]{1,0:T(8,128)(2,1)} %get-tuple-element.5) | copy-start | bytes 98308

commit v4 on v3

--- a/solution.py
+++ b/solution.py
@@ -83,7 +83,6 @@
     ext,
     mixed,
     proj,
-    mixer,
     tokens,
     hot,
     picked,
@@ -95,7 +94,6 @@
     ry2,
     home,
     result,
-    answer,
     hidden,
     w_hi,
     w_lo,
@@ -411,8 +409,6 @@
             cols = slice(k * LANE, (k + 1) * LANE)
             mixed[:, cols] = (mix * scale * group_gain[:, cols]).astype(BF)
 
-    store = pltpu.make_async_copy(mixer, mixer_out, own_s.at[2])
-
     def pool_out():
         gather["swap"].wait_recv()
         acc = jnp.zeros((rows_a, LANE), F32)
@@ -427,8 +423,7 @@
         scale = lax.rsqrt(jnp.sum(acc, axis=1, keepdims=True) * (1.0 / model) + norm_eps)
         for n in range(model // tile):
             cols = slice(n * tile, (n + 1) * tile)
-            mixer[:, cols] = (proj[:, cols] * scale * out_gain[:, cols]).astype(BF)
-        store.start()
+            mixer_out[:, cols] = (proj[:, cols] * scale * out_gain[:, cols]).astype(BF)
 
     def weigh():
         for e in range(0, experts, LANE // CAP):
@@ -578,14 +573,11 @@
     for name, *where in ORDER:
         steps[name](*where)
 
-    store.wait()
     own_back.wait()
     ref = result.at[pl.ds(0, slots - CAP)]
     pltpu.make_async_copy(ref, ref, back_r.at[0]).wait()
     value = dot(w_hi[...], result[...]) + dot(w_lo[...], result[...])
-    answer[...] = value.astype(BF)
-    last = pltpu.make_async_copy(answer, expert_out, own_s.at[3])
-    last.start()
+    expert_out[...] = value.astype(BF)
     for ref, sem in (
         (full.at[:, 0 : 3 * LANE + 3 * wide], ag_s.at[0]),
         (part.at[:, 0 : 3 * LANE + 3 * wide], rs_s.at[0]),
@@ -600,7 +592,6 @@
     pltpu.make_async_copy(ref, ref, z_s.at[0]).wait()
     ref = home.at[pl.ds(0, slots - CAP)]
     pltpu.make_async_copy(ref, ref, back_s.at[0]).wait()
-    last.wait()
 
 
 def per_device(
@@ -624,16 +615,17 @@
     slots = NZ * NC * CAP
     wide = NY * LANE
     any_ = pl.BlockSpec(memory_space=pl.ANY)
+    vmem = pl.BlockSpec(memory_space=pltpu.VMEM)
     dma = pltpu.SemaphoreType.DMA
     return pl.pallas_call(
         kernel,
         name="mixer_and_experts",
         out_shape=(
-            jax.ShapeDtypeStruct((rows_a, model), BF),
-            jax.ShapeDtypeStruct((rows_b, LANE), BF),
+            pltpu.VMEM((rows_a, model), BF),
+            pltpu.VMEM((rows_b, LANE), BF),
         ),
         in_specs=[any_] * 12,
-        out_specs=(any_, any_),
+        out_specs=(vmem, vmem),
         scratch_shapes=[
             pltpu.VMEM(pool_weight.shape, BF),
             pltpu.VMEM((1, width), F32),
@@ -648,7 +640,6 @@
             pltpu.VMEM((rows_a + RIM, width), BF),
             pltpu.VMEM((rows_a, width), BF),
             pltpu.VMEM((rows_a, model), F32),
-            pltpu.VMEM((rows_a, model), BF),
             pltpu.VMEM((rows_b, model), BF),
             pltpu.VMEM((slots, rows_b), BF),
             pltpu.VMEM((slots, LANE), BF),
@@ -660,7 +651,6 @@
             pltpu.VMEM((slots, 2 * LANE), BF),
             pltpu.VMEM((slots, LANE), BF),
             pltpu.VMEM((slots, LANE), BF),
-            pltpu.VMEM((rows_b, LANE), BF),
             pltpu.VMEM((slots, hid), BF),
             pltpu.VMEM((rows_b, slots), BF),
             pltpu.VMEM((rows_b, slots), BF),
@@ -674,7 +664,7 @@
             dma((CHUNKS,)),
             dma((1,)),
             dma((1,)),
-            dma((4,)),
+            dma((2,)),
             dma((11,)),
         ],
         compiler_params=pltpu.CompilerParams(collective_id=0, has_side_effects=True),

time: 89.7 us -> 87.7 us (0.978)
  local copies, waits for them, and re-layouts: 2.93 us -> 1.59 us
    unnamed x4 -> x2, local copies, waits for them, and re-layouts: 2.93 us -> 1.59 us
where the time goes in v4:
time: 87.7 us; the launch traced here: 87.5 us
  Pallas kernels  85.3 us (97%)
  local copies, waits for them, and re-layouts  1.59 us (2%)
    pallas_call x1, Pallas kernels, per_device(): pl.pallas_call(kernel, name='mixer_and_experts', out_shape=(pltpu.VMEM((r...  85.3 us

profile of v4, /device:TPU:1, one launch (start us, length us, event | category | flops | bytes accessed | tf_op | source)
XLA Modules:
  0.0 87.5 jit_solution(17724714473643968515)
XLA Ops:
  0.6 85.3 %mixer_and_experts.1 = (bf16[256,2048]{1,0:T(8,128)(2,1)S(1)}, bf16[128,128]{1,0:T(8,128)(2,1)S(1)}) custom-call(bf16[256,512]{1,0:T(8,128)(2,1)} %branch.1, bf16[4,128,128]{2,1,0:T(8,128)(2,1)} %pool_w_h.1, f32[1,512]{1,0:T(1,128)} %bitcast.7, bf16[512,128]{1,0:T(8,128)(2,1)} %out_w.1, f32[1,2048]{1,0:T(1,128)} %bitcast.5, bf16[128,2048]{1,0:T(8,128)(2,1)} %ffn_in.1, ...), custom_call_target="tpu_custom_call" | custom-call | tf_op jit(solution)/shard_map/mixer_and_experts/pallas_call | solution.py:620
  86.0 1.0 %copy.16 = bf16[256,2048]{1,0:T(8,128)(2,1)} copy(bf16[256,2048]{1,0:T(8,128)(2,1)S(1)} %get-tuple-element.2) | data formatting | bytes 2097152
  86.9 0.6 copy.17

commit v5 on v4

--- a/solution.py
+++ b/solution.py
@@ -31,23 +31,22 @@
 WZ = 4
 BACK = 1
 ORDER = (
-    ("ag1", 0), ("ag1", 1), ("ag2", 0, 0), ("ag2", 0, 1), ("ag1", 2), ("ag2", 1, 0), ("ag2", 1, 1), ("w2",),
-    ("ag3", 0), ("ag1", 3), ("ag1", 4), ("ag2", 2, 0), ("ag2", 2, 1), ("ag3", 1), ("ag1", 5), ("ag4", 0, 0),
-    ("ag4", 0, 1), ("ag1", 6), ("ag1", 7), ("ag2", 3, 0), ("ag2", 3, 1), ("ag3", 2), ("ag4", 1, 0),
-    ("ag4", 1, 1), ("pm",), ("ag2", 5, 0), ("ag2", 5, 1), ("w3",), ("ag2", 6, 0), ("ag2", 6, 1),
-    ("ag2", 4, 0), ("ag3", 3), ("ag2", 7, 0), ("ag2", 7, 1), ("ag2", 4, 1), ("ag3", 5), ("ag4", 2, 0),
-    ("ag4", 2, 1), ("ag3", 6), ("ag4", 3, 1), ("ag4", 3, 0), ("ag3", 7), ("ag3", 4), ("c1", 1),
-    ("ag4", 5, 0), ("c1", 0), ("ag4", 5, 1), ("c2", 0), ("w4",), ("c2", 1), ("ag4", 6, 0), ("ag4", 6, 1),
-    ("ag4", 7, 0), ("ag4", 7, 1), ("ag4", 4, 0), ("ag4", 4, 1), ("c1", 3), ("c2", 3), ("rs2", 0, 0),
-    ("rs2", 0, 1), ("c1", 5), ("c2", 5), ("c1", 7), ("c2", 7), ("c1", 6), ("rs2", 3, 0), ("rs2", 3, 1),
-    ("c2", 6), ("w5",), ("c1", 4), ("c2", 4), ("rs3", 0), ("c1", 2), ("c2", 2), ("rs2", 7, 0),
-    ("rs2", 7, 1), ("rs2", 6, 0), ("rs2", 6, 1), ("rs3", 3), ("rs4", 0, 0), ("rs4", 0, 1), ("rs2", 5, 0),
-    ("rs2", 5, 1), ("rs2", 4, 0), ("rs2", 4, 1), ("rs3", 7), ("rs5", 0), ("rs3", 6), ("rs4", 3, 0),
-    ("rs4", 3, 1), ("rs2", 1, 0), ("rs2", 1, 1), ("rs2", 2, 0), ("rs2", 2, 1), ("rs3", 5), ("w6",),
-    ("rs4", 6, 0), ("rs4", 6, 1), ("rs3", 4), ("rs4", 7, 0), ("rs4", 7, 1), ("rs5", 3), ("rs3", 1),
-    ("rs5", 6), ("rs4", 4, 0), ("rs4", 4, 1), ("rs3", 2), ("rs4", 5, 0), ("rs4", 5, 1), ("rs5", 7),
-    ("rs4", 1, 0), ("rs4", 1, 1), ("rs5", 4), ("rs4", 2, 0), ("rs4", 2, 1), ("rs5", 5), ("rs5", 1), ("w7",),
-    ("rs5", 2), ("po",), ("wh",),
+    ("ag1", 0), ("ag1", 1), ("ag2", 0, 1), ("ag2", 0, 0), ("ag1", 2), ("w2",), ("ag2", 1, 0), ("ag2", 1, 1),
+    ("ag3", 0), ("ag1", 3), ("ag2", 2, 0), ("ag1", 4), ("ag2", 2, 1), ("ag3", 1), ("ag1", 5), ("ag2", 3, 0),
+    ("ag4", 0, 0), ("ag4", 0, 1), ("ag1", 6), ("ag2", 3, 1), ("ag1", 7), ("ag4", 1, 0), ("ag3", 2),
+    ("ag4", 1, 1), ("pm",), ("ag2", 5, 1), ("ag2", 5, 0), ("ag2", 6, 1), ("ag2", 6, 0), ("ag3", 3), ("w3",),
+    ("ag2", 7, 1), ("ag2", 7, 0), ("ag2", 4, 1), ("ag4", 2, 1), ("ag2", 4, 0), ("ag3", 5), ("ag4", 2, 0),
+    ("ag4", 3, 1), ("ag4", 3, 0), ("ag3", 6), ("ag3", 7), ("w4",), ("c1", 1), ("ag3", 4), ("ag4", 5, 0),
+    ("c1", 0), ("ag4", 5, 1), ("c2", 0), ("c2", 1), ("ag4", 6, 0), ("ag4", 6, 1), ("ag4", 7, 1),
+    ("ag4", 7, 0), ("ag4", 4, 0), ("ag4", 4, 1), ("c1", 3), ("c2", 3), ("w5",), ("rs2", 0, 0),
+    ("rs2", 0, 1), ("c1", 5), ("c1", 7), ("c1", 6), ("rs2", 3, 0), ("c2", 5), ("rs2", 3, 1), ("c2", 6),
+    ("c1", 4), ("c2", 4), ("c2", 7), ("rs3", 0), ("c1", 2), ("rs2", 7, 0), ("rs2", 7, 1), ("rs2", 6, 0),
+    ("rs2", 6, 1), ("rs4", 0, 0), ("rs3", 3), ("rs4", 0, 1), ("rs2", 5, 0), ("c2", 2), ("rs2", 4, 1),
+    ("rs2", 4, 0), ("rs2", 5, 1), ("rs3", 6), ("rs2", 1, 1), ("rs4", 3, 1), ("rs3", 7), ("rs2", 1, 0),
+    ("rs4", 3, 0), ("rs2", 2, 0), ("rs2", 2, 1), ("rs5", 0), ("rs4", 6, 0), ("rs3", 5), ("w6",),
+    ("rs4", 6, 1), ("rs3", 4), ("rs4", 7, 1), ("rs4", 7, 0), ("rs3", 1), ("rs5", 3), ("rs3", 2), ("rs5", 6),
+    ("rs4", 4, 1), ("rs4", 5, 1), ("rs4", 5, 0), ("rs4", 4, 0), ("rs5", 7), ("rs4", 1, 0), ("rs4", 2, 1),
+    ("rs4", 1, 1), ("rs4", 2, 0), ("w7",), ("rs5", 5), ("rs5", 4), ("rs5", 2), ("rs5", 1), ("po",), ("wh",),
 )
 
 

time: 87.7 us -> 89.4 us (1.019)
  Pallas kernels: 85.3 us -> 87 us
    pallas_call x1, Pallas kernels: 85.3 us -> 87 us  [per_device(): pl.pallas_call(kernel, name='mixer_and_experts', out_shape=(pltpu.VMEM((r...]
where the time goes in v5:
time: 89.4 us; the launch traced here: 89.3 us
  Pallas kernels  87 us (97%)
  local copies, waits for them, and re-layouts  1.59 us (2%)
    pallas_call x1, Pallas kernels, per_device(): pl.pallas_call(kernel, name='mixer_and_experts', out_shape=(pltpu.VMEM((r...  87 us

profile of v5, /device:TPU:1, one launch (start us, length us, event | category | flops | bytes accessed | tf_op | source)
XLA Modules:
  0.0 89.3 jit_solution(5372779493947823429)
XLA Ops:
  0.6 87.0 %mixer_and_experts.1 = (bf16[256,2048]{1,0:T(8,128)(2,1)S(1)}, bf16[128,128]{1,0:T(8,128)(2,1)S(1)}) custom-call(bf16[256,512]{1,0:T(8,128)(2,1)} %branch.1, bf16[4,128,128]{2,1,0:T(8,128)(2,1)} %pool_w_h.1, f32[1,512]{1,0:T(1,128)} %bitcast.7, bf16[512,128]{1,0:T(8,128)(2,1)} %out_w.1, f32[1,2048]{1,0:T(1,128)} %bitcast.5, bf16[128,2048]{1,0:T(8,128)(2,1)} %ffn_in.1, ...), custom_call_target="tpu_custom_call" | custom-call | tf_op jit(solution)/shard_map/mixer_and_experts/pallas_call | solution.py:619
  87.7 1.0 %copy.16 = bf16[256,2048]{1,0:T(8,128)(2,1)} copy(bf16[256,2048]{1,0:T(8,128)(2,1)S(1)} %get-tuple-element.2) | data formatting | bytes 2097152
  88.6 0.6 copy.17
